TPU v7x, 32 devices: a whole 2x2x4 slice. The times are simulated.
32 devices in a mesh: sp: 8 (over z, x), tp: 4 (over y, core).
Axes of the slice: x: 2, y: 2, z: 4, core: 2. Of those that a mesh axis runs over, the one named last changes fastest.
Arguments:
- stream_in: bfloat16 [2048, 2048], P(('sp', 'tp')), may hold values from -6 to 6
- queries: bfloat16 [2048, 4096], P('sp', 'tp'), may hold values from -6 to 6
- key_rows: bfloat16 [2048, 4096], P('sp', 'tp'), may hold values from -6 to 6
- values: bfloat16 [2048, 8192], P('sp', 'tp'), may hold values from -6 to 6
- decay_low: bfloat16 [2048, 16], P('sp'), may hold values from -4 to 4
- decay_matrix: bfloat16 [16, 4096], P(None, 'tp'), may hold values from -1.5 to 1.5
- decay_bias: float32 [4096], P('tp')
- decay_shift: float32 [2048, 16], P('sp', 'tp'), may hold values from -1 to 0
- head_gain: float32 [512], replicated, may hold values from 0.1 to 1.9
- output_matrix: bfloat16 [8192, 2048], P('tp'), may hold values from -0.0625 to 0.0625
- feed_gain: float32 [2048], replicated, may hold values from 0.1 to 1.9
- routes: int32 [2048, 2], P('sp'), may hold values from 0 to 7, all different within a row; in each aligned block of 256 rows (0 to 255, 256 to 511, ...) at most 64 rows name the same one
- route_weights: float32 [2048, 2], P('sp'), may hold values from 0.2 to 1
- expert_gate: bfloat16 [8, 2048, 2816], P('sp', None, 'tp'), may hold values from -0.125 to 0.125
- specialist_widen: bfloat16 [8, 2048, 2816], P('sp', None, 'tp'), may hold values from -0.125 to 0.125
- expert_down: bfloat16 [8, 2816, 2048], P('sp', 'tp'), may hold values from -0.109375 to 0.109375
Outputs:
- layer_out: bfloat16 [2048, 2048], P(('sp', 'tp'))
Inputs may be any that keep to these rules, and one draw needn't show every extreme that they name: `routes`: each row names 2 different experts; within each aligned block of 256 rows no expert is named by more than 64 rows, and in every draw some expert is named by exactly 64 rows of some block.
All inputs are finite; a program needn't handle non-finite values.
Results may differ from a plain program's by a relative error of at most 0.02.
Values may be sent and summed in bfloat16 or wider, within the bound.
A program may use at most 128 MiB of HBM per device.

v0:
```python
import functools

import jax
import jax.numpy as jnp
from jax import lax
from jax.experimental import pallas as pl
from jax.experimental.pallas import tpu as pltpu
from jax.sharding import PartitionSpec as P

HK = 256
HV = 512
TOP = 2
BLK = 128
TEMPER = 16.0
EPSILON = 1e-06
HIGHEST = lax.Precision.HIGHEST
MESH = pl.DeviceIdType.MESH
F32 = jnp.float32
BF16 = jnp.bfloat16


def mm(a, b, ca, cb, precision=None):
    return lax.dot_general(
        a, b, (((ca,), (cb,)), ((), ())), preferred_element_type=F32, precision=precision
    )


def remote(src, dst, send, recv, target):
    return pltpu.make_async_remote_copy(
        src_ref=src, dst_ref=dst, send_sem=send, recv_sem=recv, device_id=target, device_id_type=MESH
    )


def scatter_sum(fill, store, src, r1, half, r2, s1, q1, s2, q2, y, c, ny, sent):
    partner = {"tp": 2 * y + 1 - c}
    width = src.shape[-1]
    sides = [(f, slice(f * width // 2, (f + 1) * width // 2)) for f in range(2)]

    def first(to, f, at):
        return remote(src.at[to, 1 - c, :, at], r1.at[to, :, at], s1.at[f, to], q1.at[f, to], partner)

    def second(to, slot, f, at):
        return remote(
            half.at[to, :, at], r2.at[slot, :, at], s2.at[f, to], q2.at[f, slot], {"tp": 2 * to + c}
        )

    for f, at in sides:
        fill(f)
        for i in range(1, ny + 1):
            copy = first(lax.rem(y + i, ny), f, at)
            copy.start()
            sent.append(copy)
    for f, at in sides:
        for i in range(1, ny):
            to = lax.rem(y + i, ny)
            first(to, f, at).wait_recv()
            half[to, :, at] = (src[to, c, :, at].astype(F32) + r1[to, :, at].astype(F32)).astype(BF16)
            copy = second(to, y, f, at)
            copy.start()
            sent.append(copy)
    for f, at in sides:
        first(y, f, at).wait_recv()
        total = src[y, c, :, at].astype(F32) + r1[y, :, at].astype(F32)
        for i in range(1, ny):
            to = lax.rem(y + i, ny)
            second(to, to, f, at).wait_recv()
            total = total + r2[to, :, at].astype(F32)
        store(at, total)


def layer_kernel(
    n, nt, hs, size, yl,
    stream, q, k, v, low, mat, bias, shift, gain, wout, fgain, routes, rweights, wgate, wup, wdown,
    out,
    ins, prior, sbuf, rbuf, cbuf, carry, tsend, trecv, dec, decall, acc, qs,
    wo, wg, wu, wd, mixed,
    prod, p1, ph, p2, mid, group, selt, wcomb, fb, rows, pb, r4, hy, r6, hb, r5, part, t1, th, t2,
    wsem, sa, ra, sd, rd, sb, rb, stt, rtt, sp1, rp1, sp2, rp2, sg, rg, sgc, rgc, sx, rx, sy, ry, sxc, rxc,
    s4, q4, s6, q6, s5, q5, st1, rt1, st2, rt2,
):
    me = lax.axis_index("sp")
    t = lax.axis_index("tp")
    y = t // 2
    c = lax.rem(t, 2)
    ny = nt // 2
    mine, team, teams = lax.rem(me, size), me // size, n // size
    first_one = team * size
    yo = y if yl > 1 else 0
    part_of = 2 * yo + c
    partner = {"tp": 2 * y + 1 - c}
    length = q.shape[0]
    heads = q.shape[1] // HK
    blocks = length // BLK
    width = stream.shape[1]
    rows_here = stream.shape[0]
    sent = []

    barrier = pltpu.get_barrier_semaphore()
    for i in range(1, n):
        pl.semaphore_signal(barrier, inc=1, device_id={"sp": lax.rem(me + i, n)}, device_id_type=MESH)
    for i in range(1, ny):
        pl.semaphore_signal(
            barrier, inc=1, device_id={"tp": 2 * lax.rem(y + i, ny) + c}, device_id_type=MESH
        )
    pl.semaphore_signal(barrier, inc=1, device_id=partner, device_id_type=MESH)

    loads = [
        pltpu.make_async_copy(wout, wo, wsem.at[0]),
        pltpu.make_async_copy(wgate.at[0], wg, wsem.at[1]),
        pltpu.make_async_copy(wup.at[0], wu, wsem.at[2]),
        pltpu.make_async_copy(wdown.at[0], wd, wsem.at[3]),
    ]
    for load in loads:
        load.start()

    row_id = lax.broadcasted_iota(jnp.int32, (BLK, BLK), 0)
    col_id = lax.broadcasted_iota(jnp.int32, (BLK, BLK), 1)
    causal = row_id >= col_id
    tril = causal.astype(F32)

    shifts = shift[...].T

    for h in range(heads):
        ks = slice(h * HK, (h + 1) * HK)
        pre = mm(low[...], mat[:, ks], 0, 0) + bias[:, ks]
        logged = (jnp.minimum(pre, 0.0) - jnp.log1p(jnp.exp(-jnp.abs(pre)))) / TEMPER + shifts[:, h : h + 1]
        whole = None
        for b in range(blocks):
            at = slice(b * BLK, (b + 1) * BLK)
            inside = mm(tril, logged[at], 1, 0, HIGHEST)
            ins[at, ks] = inside
            last = inside[BLK - 1 : BLK, :]
            whole = last if whole is None else whole + last
        dec[:, ks] = jnp.exp(whole)
    decall[mine] = dec[...]

    for h in range(heads):
        ks, vs = slice(h * HK, (h + 1) * HK), slice(h * HV, (h + 1) * HV)
        state = None
        for b in range(blocks):
            at = slice(b * BLK, (b + 1) * BLK)
            inside = ins[at, ks]
            last = inside[BLK - 1 : BLK, :]
            end = (k[at, ks].astype(F32) * jnp.exp(last - inside)).astype(BF16)
            added = mm(v[at, vs], end, 0, 0)
            state = added if state is None else state * jnp.exp(last) + added
            if b < blocks - 1:
                prior[b, :, ks] = state.astype(BF16)
        sbuf[h] = state.astype(BF16).reshape(size, HV // size, HK)
        if h == 0:
            pl.semaphore_wait(barrier, n - 1 + ny - 1 + 1)
            for i in range(1, size):
                to = lax.rem(mine + i, size)
                copy = remote(dec, decall.at[mine], sd.at[to], rd.at[mine], {"sp": first_one + to})
                copy.start()
                sent.append(copy)
        for i in range(1, size):
            to = lax.rem(mine + i, size)
            copy = remote(
                sbuf.at[h, to], rbuf.at[h, mine], sa.at[h, to], ra.at[h, mine], {"sp": first_one + to}
            )
            copy.start()
            sent.append(copy)
        rbuf[h, mine] = sbuf[h, mine]

    for i in range(1, size):
        j = lax.rem(mine + i, size)
        remote(dec, decall.at[j], sd.at[j], rd.at[j], {"sp": first_one + j}).wait_recv()
    onward = {"sp": lax.rem(me + size, n)}
    for h in range(heads):
        ks, vs = slice(h * HK, (h + 1) * HK), slice(h * HV, (h + 1) * HV)
        for i in range(1, size):
            j = lax.rem(mine + i, size)
            remote(sbuf.at[h, j], rbuf.at[h, j], sa.at[h, j], ra.at[h, j], {"sp": first_one + j}).wait_recv()
        link = remote(tsend.at[h], trecv.at[h], stt.at[h], rtt.at[h], onward)

        @pl.when(team > 0)
        def _():
            link.wait_recv()

        @pl.when(team == 0)
        def _():
            trecv[h] = jnp.zeros_like(trecv[h])

        total = trecv[h].astype(F32)
        for j in range(size):
            cbuf[h, j] = total.astype(BF16)
            total = total * decall[j][:, ks] + rbuf[h, j].astype(F32)

        @pl.when(team < teams - 1)
        def _():
            tsend[h] = total.astype(BF16)
            link.start()

        for i in range(1, size):
            j = lax.rem(mine + i, size)
            remote(
                cbuf.at[h, j], carry.at[h, mine], sb.at[h, j], rb.at[h, mine], {"sp": first_one + j}
            ).start()
        carry[h, mine] = cbuf[h, mine]

        passed = None
        for b in range(blocks):
            at = slice(b * BLK, (b + 1) * BLK)
            inside = ins[at, ks]
            last = inside[BLK - 1 : BLK, :]
            centre = last * 0.5
            qf = q[at, ks].astype(F32) * HK ** (-0.5)
            sq = (qf * jnp.exp(inside - centre)).astype(BF16)
            sk = (k[at, ks].astype(F32) * jnp.exp(centre - inside)).astype(BF16)
            scores = jnp.where(causal, mm(sq, sk, 1, 1), 0.0).astype(BF16)
            local = mm(scores, v[at, vs], 1, 0)
            full = inside if passed is None else inside + passed
            qs[at, ks] = (qf * jnp.exp(full)).astype(BF16)
            if b > 0:
                local = local + mm((qf * jnp.exp(inside)).astype(BF16), prior[b - 1, :, ks], 1, 1)
            passed = last if passed is None else passed + last
            acc[at, vs] = local

    lane = lax.broadcasted_iota(jnp.int32, (length, n), 1).astype(F32)
    named = routes[...].astype(F32).T
    shares = rweights[...].T
    first = (named[:, 0:1] == lane).astype(F32)
    second = (named[:, 1:2] == lane).astype(F32)
    earlier = (
        lax.broadcasted_iota(jnp.int32, (length, length), 0)
        > lax.broadcasted_iota(jnp.int32, (length, length), 1)
    ).astype(BF16)
    counts = mm(earlier, (first + second).astype(BF16), 1, 0)
    slot_lane = lax.broadcasted_iota(jnp.int32, (length, n * hs), 1).astype(F32)
    base = (part_of * hs).astype(F32)
    chosen = jnp.zeros((length, n * hs), F32)
    weighted = jnp.zeros((length, n * hs), F32)
    for j, mask in enumerate((first, second)):
        rank = jnp.sum(counts * mask, axis=1, keepdims=True) - base
        place = jnp.where(
            (rank >= 0) & (rank < hs), named[:, j : j + 1] * hs + rank, -1.0
        )
        hit = place == slot_lane
        chosen = chosen + jnp.where(hit, 1.0, 0.0)
        weighted = weighted + jnp.where(hit, shares[:, j : j + 1], 0.0)
    selt[...] = chosen.astype(BF16)
    wcomb[...] = weighted.astype(BF16)

    for h in range(heads):
        ks, vs = slice(h * HK, (h + 1) * HK), slice(h * HV, (h + 1) * HV)
        for i in range(1, size):
            j = lax.rem(mine + i, size)
            remote(cbuf.at[h, j], carry.at[h, j], sb.at[h, j], rb.at[h, j], {"sp": first_one + j}).wait()
        x = acc[:, vs] + mm(qs[:, ks], carry[h].reshape(HV, HK), 1, 1)
        scale = lax.rsqrt(jnp.mean(x * x, axis=-1, keepdims=True) + EPSILON)
        mixed[:, vs] = (x * scale * gain[...]).astype(BF16)

    loads[0].wait()
    tile = 256

    def project(f):
        @pl.loop(f * (width // tile // 2), (f + 1) * (width // tile // 2))
        def _(i):
            at = pl.ds(pl.multiple_of(i * tile, tile), tile)
            piece = mm(mixed[...], wo[:, at], 1, 0).astype(BF16)
            prod[:, :, :, at] = piece.reshape(ny, 2, rows_here, tile)

    def add_stream(at, total):
        mid[:, at] = stream[:, at].astype(F32) + total

    scatter_sum(project, add_stream, prod, p1, ph, p2, sp1, rp1, sp2, rp2, y, c, ny, sent)
    midstream = mid[...]
    scale = lax.rsqrt(jnp.mean(midstream * midstream, axis=-1, keepdims=True) + EPSILON)
    group[y, c] = (midstream * scale * fgain[...]).astype(BF16)

    for i in range(1, ny):
        to = lax.rem(y + i, ny)
        copy = remote(group.at[y, c], group.at[y, c], sg.at[to], rg.at[y], {"tp": 2 * to + c})
        copy.start()
        sent.append(copy)
    copy = remote(group.at[y, c], group.at[y, c], sgc.at[y], rgc.at[y], partner)
    copy.start()
    sent.append(copy)
    for i in range(1, ny):
        to = lax.rem(y + i, ny)
        remote(group.at[to, c], group.at[to, c], sg.at[to], rg.at[to], {"tp": 2 * to + c}).wait_recv()
        copy = remote(group.at[to, c], group.at[to, c], sgc.at[to], rgc.at[to], partner)
        copy.start()
        sent.append(copy)
    for i in range(ny):
        to = lax.rem(y + i, ny)
        remote(group.at[to, 1 - c], group.at[to, 1 - c], sgc.at[to], rgc.at[to], partner).wait_recv()

    @pl.loop(0, width // tile)
    def _(i):
        at = pl.ds(pl.multiple_of(i * tile, tile), tile)
        picked = mm(selt[...], group[:, :, :, at].reshape(length, tile), 0, 0)
        fb[:, :, at] = picked.astype(BF16).reshape(n, hs, tile)

    def pass_on(i):
        if i > 0:
            remote(fb.at[me], rows.at[i, part_of], sx.at[i], rx.at[i], {"sp": me_at(i)}).wait_recv()
        block = fb.at[me] if i == 0 else rows.at[i, part_of]
        for d in range(1, yl):
            copy = remote(
                block, rows.at[i, part_of], sy.at[i, d], ry.at[i, d], {"tp": 2 * lax.rem(y + d, ny) + c}
            )
            copy.start()
            sent.append(copy)
        copy = remote(block, rows.at[i, part_of], sxc.at[i, yo], rxc.at[i, yo], partner)
        copy.start()
        sent.append(copy)

    def pass_over(i):
        for d in range(1, yl):
            other = lax.rem(y + ny - d, ny)
            block = rows.at[i, 2 * other + c]
            remote(block, block, sy.at[i, d], ry.at[i, d], {"tp": 2 * other + c}).wait_recv()
            copy = remote(block, block, sxc.at[i, other], rxc.at[i, other], partner)
            copy.start()
            sent.append(copy)

    def me_at(i):
        return lax.rem(me + i, n)

    for i in range(1, n):
        to = lax.rem(me + i, n)
        copy = remote(fb.at[to], rows.at[i, part_of], sx.at[i], rx.at[i], {"sp": to})
        copy.start()
        sent.append(copy)
    parts = 2 * yl
    step = max(1, min(n, 256 // (parts * hs)))

    def experts(g):
        for i in range(g * step, (g + 1) * step):
            for d in range(yl):
                block = rows.at[i, 2 * d + 1 - c]
                remote(block, block, sxc.at[i, d], rxc.at[i, d], partner).wait_recv()
        taken = rows[g * step : (g + 1) * step].reshape(step * parts * hs, width)
        gated = mm(taken, wg[...], 1, 1)
        lifted = mm(taken, wu[...], 1, 1)
        hidden = (gated * jax.nn.sigmoid(gated) * lifted).astype(BF16)

        @pl.loop(0, width // 512)
        def _(i):
            at = pl.ds(pl.multiple_of(i * 512, 512), 512)
            piece = mm(hidden, wd[:, at], 1, 0).astype(BF16)
            pb[g * step : (g + 1) * step, :, :, :, at] = piece.reshape(step, yl, 2, hs, 512)

        for i in range(g * step, (g + 1) * step):
            for d in range(yl):
                copy = remote(pb.at[i, d, 1 - c], r4.at[i, d], s4.at[i, d], q4.at[i, d], partner)
                copy.start()
                sent.append(copy)

    pass_on(0)
    rows[0, part_of] = fb[me]
    early = min(step + 1, n - 1)
    for load in loads[1:]:
        load.wait()
    for i in range(1, n):
        pass_on(i)
        pass_over(i - 1)
        if i == early and step < n:
            experts(0)
    pass_over(n - 1)
    for g in range(1 if step < n else 0, n // step):
        experts(g)

    def over_core(i):
        for d in range(yl):
            remote(pb.at[i, d, c], r4.at[i, d], s4.at[i, d], q4.at[i, d], partner).wait_recv()
        for d in range(1, yl):
            other = lax.rem(y + d, ny)
            hy[i, other] = (pb[i, other, c].astype(F32) + r4[i, other].astype(F32)).astype(BF16)
            copy = remote(hy.at[i, other], r6.at[i, d], s6.at[i, d], q6.at[i, d], {"tp": 2 * other + c})
            copy.start()
            sent.append(copy)

    def over_y(i):
        both = pb[i, yo, c].astype(F32) + r4[i, yo].astype(F32)
        for d in range(1, yl):
            other = lax.rem(y + ny - d, ny)
            remote(hy.at[i, 0], r6.at[i, d], s6.at[i, d], q6.at[i, d], {"tp": 2 * other + c}).wait_recv()
            both = both + r6[i, d].astype(F32)
        if i == 0:
            r5[me] = both.astype(BF16)
        else:
            j = lax.rem(me + n - i, n)
            hb[i] = both.astype(BF16)
            copy = remote(hb.at[i], r5.at[me], s5.at[j], q5.at[me], {"sp": j})
            copy.start()
            sent.append(copy)

    lag = 2
    order = list(range(1, n)) + [0]
    for at_step in range(n + lag):
        if at_step < n:
            over_core(order[at_step])
        if at_step >= lag:
            over_y(order[at_step - lag])
    for i in range(1, n):
        j = lax.rem(me + n - i, n)
        remote(hb.at[i], r5.at[j], s5.at[j], q5.at[j], {"sp": j}).wait_recv()

    def combine(f):
        @pl.loop(f * (width // tile // 2), (f + 1) * (width // tile // 2))
        def _(i):
            at = pl.ds(pl.multiple_of(i * tile, tile), tile)
            piece = mm(wcomb[...], r5[:, :, at].reshape(n * hs, tile), 1, 0).astype(BF16)
            part[:, :, :, at] = piece.reshape(ny, 2, rows_here, tile)

    def add_routed(at, total):
        out[:, at] = (mid[:, at] + total).astype(BF16)

    scatter_sum(combine, add_routed, part, t1, th, t2, st1, rt1, st2, rt2, y, c, ny, sent)
    for copy in sent:
        copy.wait_send()

    @pl.when(team < teams - 1)
    def _():
        for h in range(heads):
            remote(tsend.at[h], trecv.at[h], stt.at[h], rtt.at[h], onward).wait_send()


def solution(mesh):
    n, nt = mesh.shape["sp"], mesh.shape["tp"]
    ny = nt // 2

    def body(
        stream_in, queries, key_rows, values, decay_low, decay_matrix, decay_bias, decay_shift,
        head_gain, output_matrix, feed_gain, routes, route_weights, expert_gate, specialist_widen,
        expert_down,
    ):
        length, keys = queries.shape
        vals = values.shape[1]
        rows_here, width = stream_in.shape
        hidden = expert_gate.shape[2]
        capacity = nt * max(1, TOP * length // (n * nt))
        yl = ny if capacity // nt >= 8 else 1
        hs = capacity // (2 * yl)
        size = next(x for x in (4, 2, 1) if n % x == 0)
        heads = keys // HK
        blocks = length // BLK
        vm = pltpu.VMEM
        dma = pltpu.SemaphoreType.DMA
        scratch = [
            vm((length, keys), F32), vm((max(1, blocks - 1), HV, keys), BF16),
            *[vm((heads, size, HV // size, HK), BF16)] * 4,
            *[vm((heads, HV // size, HK), BF16)] * 2,
            vm((1, keys), F32), vm((size, 1, keys), F32),
            vm((length, vals), F32), vm((length, keys), BF16),
            vm(output_matrix.shape, BF16), vm((hidden, width), BF16), vm((hidden, width), BF16),
            vm((hidden, width), BF16), vm((length, vals), BF16),
            vm((ny, 2, rows_here, width), BF16), vm((ny, rows_here, width), BF16),
            vm((ny, rows_here, width), BF16), vm((ny, rows_here, width), BF16),
            vm((rows_here, width), F32), vm((ny, 2, rows_here, width), BF16),
            vm((length, n * hs), BF16), vm((length, n * hs), BF16),
            vm((n, hs, width), BF16), vm((n, 2 * yl, hs, width), BF16),
            vm((n, yl, 2, hs, width), BF16), vm((n, yl, hs, width), BF16),
            vm((n, yl, hs, width), BF16), vm((n, yl, hs, width), BF16),
            vm((n, hs, width), BF16), vm((n, hs, width), BF16),
            vm((ny, 2, rows_here, width), BF16), vm((ny, rows_here, width), BF16),
            vm((ny, rows_here, width), BF16), vm((ny, rows_here, width), BF16),
            dma((4,)),
            dma((heads, size)), dma((heads, size)), dma((size,)), dma((size,)),
            dma((heads, size)), dma((heads, size)), dma((heads,)), dma((heads,)),
            *[dma((2, ny))] * 4, *[dma((ny,))] * 4,
            dma((n,)), dma((n,)), *[dma((n, yl))] * 4,
            *[dma((n, yl))] * 4, dma((n,)), dma((n,)),
            *[dma((2, ny))] * 4,
        ]
        near = pl.BlockSpec(memory_space=pltpu.VMEM)
        far = pl.BlockSpec(memory_space=pl.ANY)
        return pl.pallas_call(
            functools.partial(layer_kernel, n, nt, hs, size, yl),
            out_shape=jax.ShapeDtypeStruct((rows_here, width), BF16),
            in_specs=[near] * 9 + [far] + [near] * 3 + [far] * 3,
            out_specs=near,
            scratch_shapes=scratch,
            compiler_params=pltpu.CompilerParams(
                collective_id=0, has_side_effects=True, vmem_limit_bytes=64_000_000
            ),
            name="layer",
        )(
            stream_in, queries, key_rows, values, decay_low.T, decay_matrix, decay_bias.reshape(1, -1),
            decay_shift.T, head_gain.reshape(1, -1), output_matrix, feed_gain.reshape(1, -1), routes.T,
            route_weights.T, expert_gate.swapaxes(1, 2), specialist_widen.swapaxes(1, 2), expert_down,
        )

    return jax.shard_map(
        body,
        mesh=mesh,
        in_specs=(
            P(("sp", "tp"), None), P("sp", "tp"), P("sp", "tp"), P("sp", "tp"), P("sp", None),
            P(None, "tp"), P("tp"), P("sp", "tp"), P(), P("tp", None), P(), P("sp", None),
            P("sp", None), P("sp", None, "tp"), P("sp", None, "tp"), P("sp", "tp", None),
        ),
        out_specs=P(("sp", "tp"), None),
        check_vma=False,
    )
```

profile of v0, /device:TPU:1, one launch (start us, length us, event | category | flops | bytes accessed | tf_op | source)
XLA Modules:
  0.0 121.6 jit_solution(10698872036524222683)
XLA Ops:
  0.0 119.9 %layer.1 = bf16[64,2048]{1,0:T(8,128)(2,1)} custom-call(bf16[64,2048]{1,0:T(8,128)(2,1)} %stream.1, bf16[256,1024]{1,0:T(8,128)(2,1)} %q.1, bf16[256,1024]{1,0:T(8,128)(2,1)} %k.1, bf16[256,2048]{1,0:T(8,128)(2,1)} %v.1, bf16[16,256]{1,0:T(8,128)(2,1)} %bitcast.11, bf16[16,1024]{1,0:T(8,128)(2,1)} %mat.1, f32[1,1024]{1,0:T(1,128)} %bitcast.13, ...), custom_call_target="tpu_custom_call" | custom-call | tf_op jit(solution)/shard_map/layer/pallas_call | solution.py:471
  119.9 1.7 %copy.18 = bf16[64,2048]{1,0:T(8,128)(2,1)} copy(bf16[64,2048]{1,0:T(8,128)(2,1)} %layer.1) | data formatting | bytes 524288
where the time goes:
time: 122 us
  Pallas kernels  120 us (98%)
  local copies, waits for them, and re-layouts  1.67 us (1%)
    pallas_call x1, Pallas kernels, body(): pl.pallas_call(functools.partial(layer_kernel, n, nt, hs, size, yl), out_...  120 us

commit v1 on v0

v1 whole, which is shorter than its diff:
```python
import functools

import jax
import jax.numpy as jnp
from jax import lax
from jax.experimental import pallas as pl
from jax.experimental.pallas import tpu as pltpu
from jax.sharding import PartitionSpec as P

HK = 256
HV = 512
TOP = 2
BLK = 128
TEMPER = 16.0
EPSILON = 1e-06
HIGHEST = lax.Precision.HIGHEST
MESH = pl.DeviceIdType.MESH
F32 = jnp.float32
BF16 = jnp.bfloat16


def mm(a, b, ca, cb, precision=None):
    return lax.dot_general(
        a, b, (((ca,), (cb,)), ((), ())), preferred_element_type=F32, precision=precision
    )


def remote(src, dst, send, recv, target):
    return pltpu.make_async_remote_copy(
        src_ref=src, dst_ref=dst, send_sem=send, recv_sem=recv, device_id=target, device_id_type=MESH
    )


def layer_kernel(
    n, nt, cap, size,
    stream, q, k, v, low, mat, bias, shift, gain, wout, fgain, routes, rweights, wgate, wup, wdown,
    out,
    ins, prior, sbuf, rbuf, cbuf, carry, tsend, trecv, dec, decall, acc, qs,
    wo, wg, wu, wd, mixed,
    scols, prod, p1, ph, p2, mid, squares, selt, wcomb, sca, scb,
    fb, rows, pb, r4, hy, r6, hb, r5, outc, fin,
    wsem, sa, ra, sd, rd, sb, rb, stt, rtt, sst, rst, sp1, rp1, sp2, rp2, su, ru, ssc, rsc,
    sx, rx, sy, ry, sxc, rxc, s4, q4, s6, q6, s5, q5, sf, rf,
):
    me = lax.axis_index("sp")
    t = lax.axis_index("tp")
    y = t // 2
    c = lax.rem(t, 2)
    ny = nt // 2
    mine, team, teams = lax.rem(me, size), me // size, n // size
    first_one = team * size
    partner = {"tp": 2 * y + 1 - c}
    length = q.shape[0]
    heads = q.shape[1] // HK
    blocks = length // BLK
    width = stream.shape[1]
    rows_here = stream.shape[0]
    cw = width // nt
    tile = min(256, cw)
    sides = [slice(f * tile, (f + 1) * tile) for f in range(cw // tile)]
    sent = []

    def send(*args):
        copy = remote(*args)
        copy.start()
        sent.append(copy)

    def columns(p, f=0, wide=tile):
        return pl.ds(pl.multiple_of(p * cw + f * tile, tile), wide)

    barrier = pltpu.get_barrier_semaphore()
    for i in range(1, n):
        pl.semaphore_signal(barrier, inc=1, device_id={"sp": lax.rem(me + i, n)}, device_id_type=MESH)
    for i in range(1, nt):
        pl.semaphore_signal(barrier, inc=1, device_id={"tp": lax.rem(t + i, nt)}, device_id_type=MESH)

    loads = [
        pltpu.make_async_copy(wout, wo, wsem.at[0]),
        pltpu.make_async_copy(wgate.at[0], wg, wsem.at[1]),
        pltpu.make_async_copy(wup.at[0], wu, wsem.at[2]),
        pltpu.make_async_copy(wdown.at[0], wd, wsem.at[3]),
    ]
    for load in loads:
        load.start()

    row_id = lax.broadcasted_iota(jnp.int32, (BLK, BLK), 0)
    col_id = lax.broadcasted_iota(jnp.int32, (BLK, BLK), 1)
    causal = row_id >= col_id
    tril = causal.astype(F32)

    shifts = shift[...].T

    for h in range(heads):
        ks = slice(h * HK, (h + 1) * HK)
        pre = mm(low[...], mat[:, ks], 0, 0) + bias[:, ks]
        logged = (jnp.minimum(pre, 0.0) - jnp.log1p(jnp.exp(-jnp.abs(pre)))) / TEMPER + shifts[:, h : h + 1]
        whole = None
        for b in range(blocks):
            at = slice(b * BLK, (b + 1) * BLK)
            inside = mm(tril, logged[at], 1, 0, HIGHEST)
            ins[at, ks] = inside
            last = inside[BLK - 1 : BLK, :]
            whole = last if whole is None else whole + last
        dec[:, ks] = jnp.exp(whole)
    decall[mine] = dec[...]

    for h in range(heads):
        ks, vs = slice(h * HK, (h + 1) * HK), slice(h * HV, (h + 1) * HV)
        state = None
        for b in range(blocks):
            at = slice(b * BLK, (b + 1) * BLK)
            inside = ins[at, ks]
            last = inside[BLK - 1 : BLK, :]
            end = (k[at, ks].astype(F32) * jnp.exp(last - inside)).astype(BF16)
            added = mm(v[at, vs], end, 0, 0)
            state = added if state is None else state * jnp.exp(last) + added
            if b < blocks - 1:
                prior[b, :, ks] = state.astype(BF16)
        sbuf[h] = state.astype(BF16).reshape(size, HV // size, HK)
        if h == 0:
            pl.semaphore_wait(barrier, n - 1 + nt - 1)
            for i in range(1, size):
                to = lax.rem(mine + i, size)
                copy = remote(dec, decall.at[mine], sd.at[to], rd.at[mine], {"sp": first_one + to})
                copy.start()
                sent.append(copy)
        for i in range(1, size):
            to = lax.rem(mine + i, size)
            copy = remote(
                sbuf.at[h, to], rbuf.at[h, mine], sa.at[h, to], ra.at[h, mine], {"sp": first_one + to}
            )
            copy.start()
            sent.append(copy)
        rbuf[h, mine] = sbuf[h, mine]

    for i in range(1, nt):
        to = lax.rem(t + i, nt)
        send(stream.at[:, columns(to, 0, cw)], scols.at[t], sst.at[to], rst.at[t], {"tp": to})
    scols[t] = stream[:, columns(t, 0, cw)]

    for i in range(1, size):
        j = lax.rem(mine + i, size)
        remote(dec, decall.at[j], sd.at[j], rd.at[j], {"sp": first_one + j}).wait_recv()
    onward = {"sp": lax.rem(me + size, n)}
    for h in range(heads):
        ks, vs = slice(h * HK, (h + 1) * HK), slice(h * HV, (h + 1) * HV)
        for i in range(1, size):
            j = lax.rem(mine + i, size)
            remote(sbuf.at[h, j], rbuf.at[h, j], sa.at[h, j], ra.at[h, j], {"sp": first_one + j}).wait_recv()
        link = remote(tsend.at[h], trecv.at[h], stt.at[h], rtt.at[h], onward)

        @pl.when(team > 0)
        def _():
            link.wait_recv()

        @pl.when(team == 0)
        def _():
            trecv[h] = jnp.zeros_like(trecv[h])

        total = trecv[h].astype(F32)
        for j in range(size):
            cbuf[h, j] = total.astype(BF16)
            total = total * decall[j][:, ks] + rbuf[h, j].astype(F32)

        @pl.when(team < teams - 1)
        def _():
            tsend[h] = total.astype(BF16)
            link.start()

        for i in range(1, size):
            j = lax.rem(mine + i, size)
            remote(
                cbuf.at[h, j], carry.at[h, mine], sb.at[h, j], rb.at[h, mine], {"sp": first_one + j}
            ).start()
        carry[h, mine] = cbuf[h, mine]

        passed = None
        for b in range(blocks):
            at = slice(b * BLK, (b + 1) * BLK)
            inside = ins[at, ks]
            last = inside[BLK - 1 : BLK, :]
            centre = last * 0.5
            qf = q[at, ks].astype(F32) * HK ** (-0.5)
            sq = (qf * jnp.exp(inside - centre)).astype(BF16)
            sk = (k[at, ks].astype(F32) * jnp.exp(centre - inside)).astype(BF16)
            scores = jnp.where(causal, mm(sq, sk, 1, 1), 0.0).astype(BF16)
            local = mm(scores, v[at, vs], 1, 0)
            full = inside if passed is None else inside + passed
            qs[at, ks] = (qf * jnp.exp(full)).astype(BF16)
            if b > 0:
                local = local + mm((qf * jnp.exp(inside)).astype(BF16), prior[b - 1, :, ks], 1, 1)
            passed = last if passed is None else passed + last
            acc[at, vs] = local

    lane = lax.broadcasted_iota(jnp.int32, (length, n), 1).astype(F32)
    named = routes[...].astype(F32).T
    shares = rweights[...].T
    first_named = (named[:, 0:1] == lane).astype(F32)
    second_named = (named[:, 1:2] == lane).astype(F32)
    earlier = (
        lax.broadcasted_iota(jnp.int32, (length, length), 0)
        > lax.broadcasted_iota(jnp.int32, (length, length), 1)
    ).astype(BF16)
    counts = mm(earlier, (first_named + second_named).astype(BF16), 1, 0)
    slot_lane = lax.broadcasted_iota(jnp.int32, (length, n * cap), 1).astype(F32)
    chosen = jnp.zeros((length, n * cap), F32)
    weighted = jnp.zeros((length, n * cap), F32)
    for j, mask in enumerate((first_named, second_named)):
        rank = jnp.sum(counts * mask, axis=1, keepdims=True)
        place = jnp.where(rank < cap, named[:, j : j + 1] * cap + rank, -1.0)
        hit = place == slot_lane
        chosen = chosen + jnp.where(hit, 1.0, 0.0)
        weighted = weighted + jnp.where(hit, shares[:, j : j + 1], 0.0)
    selt[...] = chosen.T.astype(BF16)
    wcomb[...] = weighted.astype(BF16)
    sca[...] = jnp.zeros_like(sca)

    for h in range(heads):
        ks, vs = slice(h * HK, (h + 1) * HK), slice(h * HV, (h + 1) * HV)
        for i in range(1, size):
            j = lax.rem(mine + i, size)
            remote(cbuf.at[h, j], carry.at[h, j], sb.at[h, j], rb.at[h, j], {"sp": first_one + j}).wait()
        x = acc[:, vs] + mm(qs[:, ks], carry[h].reshape(HV, HK), 1, 1)
        scale = lax.rsqrt(jnp.mean(x * x, axis=-1, keepdims=True) + EPSILON)
        mixed[:, vs] = (x * scale * gain[...]).astype(BF16)

    loads[0].wait()

    def first(to, f):
        at = sides[f]
        return remote(
            prod.at[to, 1 - c, :, at], p1.at[to, :, at], sp1.at[f, to], rp1.at[f, to], partner
        )

    def second(to, slot, f):
        at = sides[f]
        return remote(
            ph.at[to, :, at], p2.at[slot, :, at], sp2.at[f, to], rp2.at[f, slot], {"tp": 2 * to + c}
        )

    def project(to, core, f):
        prod[to, core, :, sides[f]] = mm(mixed[...], wo[:, columns(2 * to + core, f)], 1, 0).astype(BF16)

    for i in range(1, ny + 1):
        to = lax.rem(y + i, ny)
        for f in range(len(sides)):
            project(to, 1 - c, f)
            copy = first(to, f)
            copy.start()
            sent.append(copy)
        for f in range(len(sides)):
            project(to, c, f)
        if i < ny:
            for f, at in enumerate(sides):
                first(to, f).wait_recv()
                ph[to, :, at] = (prod[to, c, :, at].astype(F32) + p1[to, :, at].astype(F32)).astype(BF16)
                copy = second(to, y, f)
                copy.start()
                sent.append(copy)

    for i in range(1, nt):
        p = lax.rem(t + i, nt)
        remote(scols.at[p], scols.at[p], sst.at[p], rst.at[p], {"tp": p}).wait_recv()
    square = jnp.zeros((length, 1), F32)
    for f, at in enumerate(sides):
        first(y, f).wait_recv()
        total = prod[y, c, :, at].astype(F32) + p1[y, :, at].astype(F32)
        for i in range(1, ny):
            to = lax.rem(y + i, ny)
            second(to, to, f).wait_recv()
            total = total + p2[to, :, at].astype(F32)
        x = scols[:, :, at].reshape(length, tile).astype(F32) + total
        mid[:, at] = x
        square = square + jnp.sum(x * x, axis=1, keepdims=True)
        picked = mm(selt[...], (x * fgain[:, columns(t, f)]).astype(BF16), 1, 0)
        fb[:, :, at] = picked.astype(BF16).reshape(n, cap, tile)

    def pass_on(i):
        if i > 0:
            remote(fb.at[me], rows.at[i, t], sx.at[i], rx.at[i], {"sp": me}).wait_recv()
        block = fb.at[me] if i == 0 else rows.at[i, t]
        for d in range(1, ny):
            send(block, rows.at[i, t], sy.at[i, d], ry.at[i, d], {"tp": 2 * lax.rem(y + d, ny) + c})
        send(block, rows.at[i, t], sxc.at[i, y], rxc.at[i, y], partner)

    def pass_over(i):
        for d in range(1, ny):
            other = lax.rem(y + ny - d, ny)
            block = rows.at[i, 2 * other + c]
            remote(block, block, sy.at[i, d], ry.at[i, d], {"tp": 2 * other + c}).wait_recv()
            send(block, block, sxc.at[i, other], rxc.at[i, other], partner)

    for i in range(1, n):
        to = lax.rem(me + i, n)
        send(fb.at[to], rows.at[i, t], sx.at[i], rx.at[i], {"sp": to})
    squares[t] = jnp.broadcast_to(square, (length, 128)).T[0:1, :]
    for i in range(1, nt):
        p = lax.rem(t + i, nt)
        send(squares.at[t], squares.at[t], su.at[p], ru.at[t], {"tp": p})

    def row_scales():
        total = squares[t]
        for i in range(1, nt):
            p = lax.rem(t + i, nt)
            remote(squares.at[p], squares.at[p], su.at[p], ru.at[p], {"tp": p}).wait_recv()
            total = total + squares[p]
        scale = lax.rsqrt(total / width + EPSILON)
        high = scale.astype(BF16).astype(F32)
        middle = (scale - high).astype(BF16).astype(F32)
        third = scale - high - middle
        line = lax.broadcasted_iota(jnp.int32, (8, length), 0)
        parts = jnp.where(line == 0, high, jnp.where(line == 1, middle, jnp.where(line == 2, third, 0.0)))
        slot_scale = jnp.sum(mm(parts.astype(BF16), selt[...], 1, 1), axis=0, keepdims=True)
        for e in range(n):
            sca[e, :, 0:cap] = slot_scale[:, e * cap : (e + 1) * cap]
        for i in range(1, n):
            to = lax.rem(me + i, n)
            send(sca.at[to], scb.at[i], ssc.at[i], rsc.at[i], {"sp": to})
        scb[0] = sca[me]

    step = max(1, min(n, 256 // cap))

    def experts(g):
        group = range(g * step, (g + 1) * step)
        span = slice(g * step, (g + 1) * step)
        scales = []
        for i in group:
            for d in range(ny):
                block = rows.at[i, 2 * d + 1 - c]
                remote(block, block, sxc.at[i, d], rxc.at[i, d], partner).wait_recv()
            if i > 0:
                remote(sca.at[me], scb.at[i], ssc.at[i], rsc.at[i], {"sp": me}).wait_recv()
            scales.append(jnp.broadcast_to(scb[i], (8, 128)).T[0:cap, 0:1])
        scale = jnp.concatenate(scales, axis=0)
        taken = jnp.concatenate([rows[span, p].reshape(step * cap, cw) for p in range(nt)], axis=1)
        gated = mm(taken, wg[...], 1, 1) * scale
        lifted = mm(taken, wu[...], 1, 1) * scale
        hidden = (gated * jax.nn.sigmoid(gated) * lifted).astype(BF16)
        for core in (1 - c, c):
            @pl.loop(0, ny)
            def _(d):
                piece = mm(hidden, wd[:, columns(2 * d + core, 0, cw)], 1, 0).astype(BF16)
                pb[span, d, core] = piece.reshape(step, cap, cw)

            if core is not c:
                for i in group:
                    for d in range(ny):
                        send(pb.at[i, d, core], r4.at[i, d], s4.at[i, d], q4.at[i, d], partner)

    def over_core(i):
        for d in range(ny):
            remote(pb.at[i, d, c], r4.at[i, d], s4.at[i, d], q4.at[i, d], partner).wait_recv()
        for d in range(1, ny):
            other = lax.rem(y + d, ny)
            hy[i, other] = (pb[i, other, c].astype(F32) + r4[i, other].astype(F32)).astype(BF16)
            send(hy.at[i, other], r6.at[i, d], s6.at[i, d], q6.at[i, d], {"tp": 2 * other + c})

    def over_y(i):
        both = pb[i, y, c].astype(F32) + r4[i, y].astype(F32)
        for d in range(1, ny):
            other = lax.rem(y + ny - d, ny)
            remote(hy.at[i, 0], r6.at[i, d], s6.at[i, d], q6.at[i, d], {"tp": 2 * other + c}).wait_recv()
            both = both + r6[i, d].astype(F32)
        if i == 0:
            r5[me] = both.astype(BF16)
        else:
            j = lax.rem(me + n - i, n)
            hb[i] = both.astype(BF16)
            send(hb.at[i], r5.at[me], s5.at[j], q5.at[me], {"sp": j})

    pass_on(0)
    rows[0, t] = fb[me]
    early = min(step + 1, n - 1)
    for load in loads[1:]:
        load.wait()
    for i in range(1, n):
        pass_on(i)
        pass_over(i - 1)
        if i == min(2, n - 1):
            row_scales()
        if i == early and step < n:
            experts(0)
    pass_over(n - 1)
    order = list(range(1, n)) + [0]
    ahead = 0
    if step < n:
        for i in range(1, step):
            over_core(i)
        ahead = step - 1
    for g in range(1 if step < n else 0, n // step):
        experts(g)

    lag = 2 + ahead
    for at_step in range(ahead, n + lag):
        if at_step < n:
            over_core(order[at_step])
        if at_step >= lag:
            over_y(order[at_step - lag])
    for i in range(1, n):
        j = lax.rem(me + n - i, n)
        remote(hb.at[i], r5.at[j], s5.at[j], q5.at[j], {"sp": j}).wait_recv()

    finished = mid[...] + mm(wcomb[...], r5[...].reshape(n * cap, cw), 1, 0)
    outc[...] = finished.astype(BF16).reshape(nt, rows_here, cw)
    for i in range(1, nt):
        p = lax.rem(t + i, nt)
        send(outc.at[p], fin.at[t], sf.at[p], rf.at[t], {"tp": p})
    fin[t] = outc[t]
    for i in range(1, nt):
        p = lax.rem(t + i, nt)
        remote(outc.at[p], fin.at[p], sf.at[p], rf.at[p], {"tp": p}).wait_recv()
    for p in range(nt):
        out[:, p * cw : (p + 1) * cw] = fin[p]
    for copy in sent:
        copy.wait_send()

    @pl.when(team < teams - 1)
    def _():
        for h in range(heads):
            remote(tsend.at[h], trecv.at[h], stt.at[h], rtt.at[h], onward).wait_send()


def solution(mesh):
    n, nt = mesh.shape["sp"], mesh.shape["tp"]
    ny = nt // 2

    def body(
        stream_in, queries, key_rows, values, decay_low, decay_matrix, decay_bias, decay_shift,
        head_gain, output_matrix, feed_gain, routes, route_weights, expert_gate, specialist_widen,
        expert_down,
    ):
        length, keys = queries.shape
        vals = values.shape[1]
        rows_here, width = stream_in.shape
        hidden = expert_gate.shape[2]
        cap = nt * max(1, TOP * length // (n * nt))
        cw = width // nt
        sides = cw // min(256, cw)
        size = next(x for x in (4, 2, 1) if n % x == 0)
        heads = keys // HK
        blocks = length // BLK
        vm = pltpu.VMEM
        dma = pltpu.SemaphoreType.DMA
        scratch = [
            vm((length, keys), F32), vm((max(1, blocks - 1), HV, keys), BF16),
            *[vm((heads, size, HV // size, HK), BF16)] * 4,
            *[vm((heads, HV // size, HK), BF16)] * 2,
            vm((1, keys), F32), vm((size, 1, keys), F32),
            vm((length, vals), F32), vm((length, keys), BF16),
            vm(output_matrix.shape, BF16), vm((hidden, width), BF16), vm((hidden, width), BF16),
            vm((hidden, width), BF16), vm((length, vals), BF16),
            vm((nt, rows_here, cw), BF16), vm((ny, 2, length, cw), BF16), *[vm((ny, length, cw), BF16)] * 3,
            vm((length, cw), F32), vm((nt, 1, length), F32),
            vm((n * cap, length), BF16), vm((length, n * cap), BF16),
            vm((n, 1, 128), F32), vm((n, 1, 128), F32),
            vm((n, cap, cw), BF16), vm((n, nt, cap, cw), BF16),
            vm((n, ny, 2, cap, cw), BF16), *[vm((n, ny, cap, cw), BF16)] * 3,
            vm((n, cap, cw), BF16), vm((n, cap, cw), BF16),
            vm((nt, rows_here, cw), BF16), vm((nt, rows_here, cw), BF16),
            dma((4,)),
            dma((heads, size)), dma((heads, size)), dma((size,)), dma((size,)),
            dma((heads, size)), dma((heads, size)), dma((heads,)), dma((heads,)),
            dma((nt,)), dma((nt,)), *[dma((sides, ny))] * 4,
            dma((nt,)), dma((nt,)), dma((n,)), dma((n,)),
            dma((n,)), dma((n,)), *[dma((n, ny))] * 4,
            *[dma((n, ny))] * 4, dma((n,)), dma((n,)),
            dma((nt,)), dma((nt,)),
        ]
        near = pl.BlockSpec(memory_space=pltpu.VMEM)
        far = pl.BlockSpec(memory_space=pl.ANY)
        return pl.pallas_call(
            functools.partial(layer_kernel, n, nt, cap, size),
            out_shape=jax.ShapeDtypeStruct((rows_here, width), BF16),
            in_specs=[near] * 9 + [far] + [near] * 3 + [far] * 3,
            out_specs=near,
            scratch_shapes=scratch,
            compiler_params=pltpu.CompilerParams(
                collective_id=0, has_side_effects=True, vmem_limit_bytes=64_000_000
            ),
            name="layer",
        )(
            stream_in, queries, key_rows, values, decay_low.T, decay_matrix, decay_bias.reshape(1, -1),
            decay_shift.T, head_gain.reshape(1, -1), output_matrix, feed_gain.reshape(1, -1), routes.T,
            route_weights.T, expert_gate.swapaxes(1, 2), specialist_widen.swapaxes(1, 2), expert_down,
        )

    return jax.shard_map(
        body,
        mesh=mesh,
        in_specs=(
            P(("sp", "tp"), None), P("sp", "tp"), P("sp", "tp"), P("sp", "tp"), P("sp", None),
            P(None, "tp"), P("tp"), P("sp", "tp"), P(), P("tp", None), P(), P("sp", None),
            P("sp", None), P("sp", None, "tp"), P("sp", None, "tp"), P("sp", "tp", None),
        ),
        out_specs=P(("sp", "tp"), None),
        check_vma=False,
    )
```

time: 122 us -> 102 us (0.84)
  Pallas kernels: 120 us -> 99.8 us
    pallas_call x1, Pallas kernels: 120 us -> 99.8 us  [body(): pl.pallas_call(functools.partial(layer_kernel, n, nt, cap, size), out_sha...]
where the time goes in v1:
time: 102 us; the launch traced here: 101 us
  Pallas kernels  99.8 us (98%)
  local copies, waits for them, and re-layouts  1.67 us (2%)
    pallas_call x1, Pallas kernels, body(): pl.pallas_call(functools.partial(layer_kernel, n, nt, cap, size), out_sha...  99.8 us

profile of v1, /device:TPU:1, one launch (start us, length us, event | category | flops | bytes accessed | tf_op | source)
XLA Modules:
  0.0 101.5 jit_solution(10786152598211050808)
XLA Ops:
  0.0 99.8 %layer.1 = bf16[64,2048]{1,0:T(8,128)(2,1)} custom-call(bf16[64,2048]{1,0:T(8,128)(2,1)} %stream.1, bf16[256,1024]{1,0:T(8,128)(2,1)} %q.1, bf16[256,1024]{1,0:T(8,128)(2,1)} %k.1, bf16[256,2048]{1,0:T(8,128)(2,1)} %v.1, bf16[16,256]{1,0:T(8,128)(2,1)} %bitcast.11, bf16[16,1024]{1,0:T(8,128)(2,1)} %mat.1, f32[1,1024]{1,0:T(1,128)} %bitcast.13, ...), custom_call_target="tpu_custom_call" | custom-call | tf_op jit(solution)/shard_map/layer/pallas_call | solution.py:471
  99.8 1.7 %copy.18 = bf16[64,2048]{1,0:T(8,128)(2,1)} copy(bf16[64,2048]{1,0:T(8,128)(2,1)} %layer.1) | data formatting | bytes 524288

commit v2 on v1

v2 whole, which is shorter than its diff:
```python
import functools

import jax
import jax.numpy as jnp
from jax import lax
from jax.experimental import pallas as pl
from jax.experimental.pallas import tpu as pltpu
from jax.sharding import PartitionSpec as P

HK = 256
HV = 512
TOP = 2
PIECES = 4
BLK = 128
TEMPER = 16.0
EPSILON = 1e-06
HIGHEST = lax.Precision.HIGHEST
MESH = pl.DeviceIdType.MESH
F32 = jnp.float32
BF16 = jnp.bfloat16


def mm(a, b, ca, cb, precision=None):
    return lax.dot_general(
        a, b, (((ca,), (cb,)), ((), ())), preferred_element_type=F32, precision=precision
    )


def remote(src, dst, send, recv, target):
    return pltpu.make_async_remote_copy(
        src_ref=src, dst_ref=dst, send_sem=send, recv_sem=recv, device_id=target, device_id_type=MESH
    )


def layer_kernel(
    n, nt, cap, size,
    stream, q, k, v, low, mat, bias, shift, gain, wout, fgain, routes, rweights, wgate, wup, wdown,
    out,
    ins, prior, sbuf, rbuf, cbuf, carry, tsend, trecv, dec, decall, acc, qs,
    wo, wgud, mixed,
    scols, prod, p1, ph, p2, mid, squares, selt, wcomb, sca, scb,
    fb, rows, gates, hiddens, pb, r4, hy, r6, hb, r5, outc, fin,
    wsem, sa, ra, sd, rd, sb, rb, stt, rtt, sst, rst, sp1, rp1, sp2, rp2, su, ru, ssc, rsc,
    sx, rx, sy, ry, sxc, rxc, s4, q4, s6, q6, s5, q5, sf, rf,
):
    me = lax.axis_index("sp")
    t = lax.axis_index("tp")
    y = t // 2
    c = lax.rem(t, 2)
    ny = nt // 2
    mine, team, teams = lax.rem(me, size), me // size, n // size
    first_one = team * size
    partner = {"tp": 2 * y + 1 - c}
    length = q.shape[0]
    heads = q.shape[1] // HK
    blocks = length // BLK
    width = stream.shape[1]
    rows_here = stream.shape[0]
    cw = width // nt
    tile = min(256, cw)
    sides = [slice(f * tile, (f + 1) * tile) for f in range(cw // tile)]
    high = HV // size
    piece = max(16, high // PIECES)
    pieces = [slice(a, a + piece) for a in range(0, high, piece)]

    def send(*args):
        remote(*args).start()

    def arrived(ref, semaphore):
        remote(ref, ref, semaphore, semaphore, partner).wait_recv()

    def departed(ref, semaphore):
        remote(ref, ref, semaphore, semaphore, partner).wait_send()

    def columns(p, f=0, wide=tile):
        return pl.ds(pl.multiple_of(p * cw + f * tile, tile), wide)

    barrier = pltpu.get_barrier_semaphore()
    for i in range(1, n):
        pl.semaphore_signal(barrier, inc=1, device_id={"sp": lax.rem(me + i, n)}, device_id_type=MESH)
    for i in range(1, nt):
        pl.semaphore_signal(barrier, inc=1, device_id={"tp": lax.rem(t + i, nt)}, device_id_type=MESH)

    load_out = pltpu.make_async_copy(wout, wo, wsem.at[0])
    load_out.start()
    for i, weight in enumerate((wgate, wup, wdown)):
        pltpu.make_async_copy(weight.at[0], wgud.at[i], wsem.at[1]).start()

    row_id = lax.broadcasted_iota(jnp.int32, (BLK, BLK), 0)
    col_id = lax.broadcasted_iota(jnp.int32, (BLK, BLK), 1)
    causal = row_id >= col_id
    tril = causal.astype(F32)

    shifts = shift[...].T

    for h in range(heads):
        ks, vs = slice(h * HK, (h + 1) * HK), slice(h * HV, (h + 1) * HV)
        pre = mm(low[...], mat[:, ks], 0, 0) + bias[:, ks]
        logged = (jnp.minimum(pre, 0.0) - jnp.log1p(jnp.exp(-jnp.abs(pre)))) / TEMPER + shifts[:, h : h + 1]
        whole = None
        state = None
        for b in range(blocks):
            at = slice(b * BLK, (b + 1) * BLK)
            inside = mm(tril, logged[at], 1, 0, HIGHEST)
            ins[at, ks] = inside
            last = inside[BLK - 1 : BLK, :]
            whole = last if whole is None else whole + last
            end = (k[at, ks].astype(F32) * jnp.exp(last - inside)).astype(BF16)
            added = mm(v[at, vs], end, 0, 0)
            state = added if state is None else state * jnp.exp(last) + added
            if b < blocks - 1:
                prior[b, :, ks] = state.astype(BF16)
        sbuf[h] = state.astype(BF16).reshape(size, HV // size, HK)
        dec[h] = jnp.exp(whole)
        if h == 0:
            pl.semaphore_wait(barrier, n - 1 + nt - 1)
        for i in range(1, size):
            to = lax.rem(mine + i, size)
            send(dec.at[h], decall.at[h, mine], sd.at[0], rd.at[h], {"sp": first_one + to})
        for p, part in enumerate(pieces):
            for i in range(1, size):
                to = lax.rem(mine + i, size)
                send(
                    sbuf.at[h, to, part], rbuf.at[h, mine, part], sa.at[0], ra.at[h, p], {"sp": first_one + to}
                )
        rbuf[h, mine] = sbuf[h, mine]
        decall[h, mine] = dec[h]

    for i in range(1, nt):
        to = lax.rem(t + i, nt)
        send(stream.at[:, columns(to, 0, cw)], scols.at[t], sst.at[0], rst.at[0], {"tp": to})
    scols[t] = stream[:, columns(t, 0, cw)]

    onward = {"sp": lax.rem(me + size, n)}
    for h in range(heads):
        ks, vs = slice(h * HK, (h + 1) * HK), slice(h * HV, (h + 1) * HV)
        arrived(decall.at[h, 0 : size - 1], rd.at[h])
        for p, part in enumerate(pieces):
            arrived(rbuf.at[h, 0 : size - 1, part], ra.at[h, p])
            link = remote(tsend.at[h, part], trecv.at[h, part], stt.at[0], rtt.at[h, p], onward)

            @pl.when(team > 0)
            def _():
                link.wait_recv()

            @pl.when(team == 0)
            def _():
                trecv[h, part] = jnp.zeros_like(trecv[h, part])

            total = trecv[h, part].astype(F32)
            for j in range(size):
                cbuf[h, j, part] = total.astype(BF16)
                total = total * decall[h, j] + rbuf[h, j, part].astype(F32)

            @pl.when(team < teams - 1)
            def _():
                tsend[h, part] = total.astype(BF16)
                link.start()

            for i in range(1, size):
                j = lax.rem(mine + i, size)
                send(cbuf.at[h, j, part], carry.at[h, mine, part], sb.at[0], rb.at[h], {"sp": first_one + j})
        carry[h, mine] = cbuf[h, mine]

        passed = None
        for b in range(blocks):
            at = slice(b * BLK, (b + 1) * BLK)
            inside = ins[at, ks]
            last = inside[BLK - 1 : BLK, :]
            centre = last * 0.5
            qf = q[at, ks].astype(F32) * HK ** (-0.5)
            sq = (qf * jnp.exp(inside - centre)).astype(BF16)
            sk = (k[at, ks].astype(F32) * jnp.exp(centre - inside)).astype(BF16)
            scores = jnp.where(causal, mm(sq, sk, 1, 1), 0.0).astype(BF16)
            local = mm(scores, v[at, vs], 1, 0)
            full = inside if passed is None else inside + passed
            qs[at, ks] = (qf * jnp.exp(full)).astype(BF16)
            if b > 0:
                local = local + mm((qf * jnp.exp(inside)).astype(BF16), prior[b - 1, :, ks], 1, 1)
            passed = last if passed is None else passed + last
            acc[at, vs] = local
        if h == min(1, heads - 1):
            lane = lax.broadcasted_iota(jnp.int32, (length, n), 1).astype(F32)
            named = routes[...].astype(F32).T
            shares = rweights[...].T
            first_named = (named[:, 0:1] == lane).astype(F32)
            second_named = (named[:, 1:2] == lane).astype(F32)
            earlier = (
                lax.broadcasted_iota(jnp.int32, (length, length), 0)
                > lax.broadcasted_iota(jnp.int32, (length, length), 1)
            ).astype(BF16)
            counts = mm(earlier, (first_named + second_named).astype(BF16), 1, 0)
            slot_lane = lax.broadcasted_iota(jnp.int32, (length, n * cap), 1).astype(F32)
            chosen = jnp.zeros((length, n * cap), F32)
            weighted = jnp.zeros((length, n * cap), F32)
            for j, mask in enumerate((first_named, second_named)):
                rank = jnp.sum(counts * mask, axis=1, keepdims=True)
                place = jnp.where(rank < cap, named[:, j : j + 1] * cap + rank, -1.0)
                hit = place == slot_lane
                chosen = chosen + jnp.where(hit, 1.0, 0.0)
                weighted = weighted + jnp.where(hit, shares[:, j : j + 1], 0.0)
            selt[...] = chosen.T.astype(BF16)
            wcomb[...] = weighted.astype(BF16)
            sca[...] = jnp.zeros_like(sca)


    for h in range(heads):
        ks, vs = slice(h * HK, (h + 1) * HK), slice(h * HV, (h + 1) * HV)
        arrived(carry.at[h, 0 : size - 1], rb.at[h])
        x = acc[:, vs] + mm(qs[:, ks], carry[h].reshape(HV, HK), 1, 1)
        scale = lax.rsqrt(jnp.mean(x * x, axis=-1, keepdims=True) + EPSILON)
        mixed[:, vs] = (x * scale * gain[...]).astype(BF16)

    load_out.wait()

    def first(to, f):
        at = sides[f]
        return remote(
            prod.at[to, 1 - c, :, at], p1.at[to, :, at], sp1.at[0], rp1.at[f, to], partner
        )

    def second(to, slot, f):
        at = sides[f]
        return remote(
            ph.at[to, :, at], p2.at[slot, :, at], sp2.at[0], rp2.at[f, slot], {"tp": 2 * to + c}
        )

    def project(to, core, f):
        prod[to, core, :, sides[f]] = mm(mixed[...], wo[:, columns(2 * to + core, f)], 1, 0).astype(BF16)

    for i in range(1, ny + 1):
        to = lax.rem(y + i, ny)
        for f in range(len(sides)):
            project(to, 1 - c, f)
            first(to, f).start()
        for f in range(len(sides)):
            project(to, c, f)
        if i < ny:
            for f, at in enumerate(sides):
                first(to, f).wait_recv()
                ph[to, :, at] = (prod[to, c, :, at].astype(F32) + p1[to, :, at].astype(F32)).astype(BF16)
                second(to, y, f).start()

    arrived(scols.at[0 : nt - 1], rst.at[0])
    square = jnp.zeros((length, 1), F32)
    for f, at in enumerate(sides):
        first(y, f).wait_recv()
        total = prod[y, c, :, at].astype(F32) + p1[y, :, at].astype(F32)
        for i in range(1, ny):
            to = lax.rem(y + i, ny)
            second(to, to, f).wait_recv()
            total = total + p2[to, :, at].astype(F32)
        x = scols[:, :, at].reshape(length, tile).astype(F32) + total
        mid[:, at] = x
        square = square + jnp.sum(x * x, axis=1, keepdims=True)
        picked = mm(selt[...], (x * fgain[:, columns(t, f)]).astype(BF16), 1, 0)
        fb[:, :, at] = picked.astype(BF16).reshape(n, cap, tile)

    step = max(1, min(n, 256 // cap))
    groups = [range(a, a + step) for a in range(0, n, step)]
    if step > 1:
        first_half = groups[-1][: step // 2]
        groups = groups[:-1] + [first_half, groups[-1][step // 2 :]]

    def group_of(i):
        return next(g for g, group in enumerate(groups) if i in group)

    def pass_on(i):
        if i > 0:
            arrived(rows.at[i, t], rx.at[i])
        block = fb.at[me] if i == 0 else rows.at[i, t]
        for d in range(1, ny):
            send(block, rows.at[i, t], sy.at[0], ry.at[i, d - 1], {"tp": 2 * lax.rem(y + d, ny) + c})
        send(block, rows.at[i, t], sxc.at[0], rxc.at[group_of(i)], partner)

    def pass_over(i):
        for d in range(1, ny):
            other = lax.rem(y + ny - d, ny)
            block = rows.at[i, 2 * other + c]
            arrived(block, ry.at[i, d - 1])
            send(block, block, sxc.at[0], rxc.at[group_of(i)], partner)

    def dispatch(i):
        to = lax.rem(me + i, n)
        send(fb.at[to], rows.at[i, t], sx.at[0], rx.at[i], {"sp": to})

    soon = min(4, n)
    for i in range(1, soon):
        dispatch(i)
    squares[t] = jnp.broadcast_to(square, (length, 128)).T[0:1, :]
    for i in range(1, nt):
        p = lax.rem(t + i, nt)
        send(squares.at[t], squares.at[t], su.at[0], ru.at[0], {"tp": p})

    def row_scales():
        arrived(squares.at[0 : nt - 1], ru.at[0])
        total = jnp.sum(squares[...], axis=0)
        scale = lax.rsqrt(total / width + EPSILON)
        high = scale.astype(BF16).astype(F32)
        middle = (scale - high).astype(BF16).astype(F32)
        third = scale - high - middle
        line = lax.broadcasted_iota(jnp.int32, (8, length), 0)
        parts = jnp.where(line == 0, high, jnp.where(line == 1, middle, jnp.where(line == 2, third, 0.0)))
        slot_scale = jnp.sum(mm(parts.astype(BF16), selt[...], 1, 1), axis=0, keepdims=True)
        for e in range(n):
            sca[e, :, 0:cap] = slot_scale[:, e * cap : (e + 1) * cap]
        for i in range(1, n):
            to = lax.rem(me + i, n)
            send(sca.at[to], scb.at[i], ssc.at[0], rsc.at[0], {"sp": to})
        scb[0] = sca[me]

    def experts(g):
        group = groups[g]
        span = slice(group[0], group[-1] + 1)
        size_here = len(group) * cap
        arrived(rows.at[span, 0:ny], rxc.at[g])
        scales = [jnp.broadcast_to(scb[i], (8, 128)).T[0:cap, 0:1] for i in group]
        scale = jnp.concatenate(scales, axis=0)
        parts = [rows[span, p].reshape(size_here, cw) for p in range(nt)]
        gates[0:size_here] = mm(jnp.concatenate(parts, axis=1), wgud[0], 1, 1) * scale
        yield
        parts = [rows[span, p].reshape(size_here, cw) for p in range(nt)]
        lifted = mm(jnp.concatenate(parts, axis=1), wgud[1], 1, 1) * scale
        gated = gates[0:size_here]
        hiddens[0:size_here] = (gated * jax.nn.sigmoid(gated) * lifted).astype(BF16)
        yield
        for core in (1 - c, c):
            @pl.loop(0, ny)
            def _(d):
                piece = mm(hiddens[0:size_here], wgud[2, :, columns(2 * d + core, 0, cw)], 1, 0).astype(BF16)
                pb[span, d, core] = piece.reshape(len(group), cap, cw)

            if core is not c:
                for i in group:
                    for d in range(ny):
                        send(pb.at[i, d, core], r4.at[i, d], s4.at[0], q4.at[g], partner)
            yield

    def over_core(i):
        for d in range(1, ny):
            other = lax.rem(y + d, ny)
            hy[i, other] = (pb[i, other, c].astype(F32) + r4[i, other].astype(F32)).astype(BF16)
            send(hy.at[i, other], r6.at[i, d], s6.at[0], q6.at[i, d - 1], {"tp": 2 * other + c})

    def over_y(i):
        both = pb[i, y, c].astype(F32) + r4[i, y].astype(F32)
        for d in range(1, ny):
            arrived(r6.at[i, d], q6.at[i, d - 1])
            both = both + r6[i, d].astype(F32)
        if i == 0:
            r5[me] = both.astype(BF16)
        else:
            j = lax.rem(me + n - i, n)
            hb[i] = both.astype(BF16)
            send(hb.at[i], r5.at[me], s5.at[0], q5.at[0], {"sp": j})

    work, computed, returned = [], [], []

    def back(g):
        arrived(r4.at[groups[g][0] : groups[g][-1] + 1], q4.at[g])
        for i in groups[g]:
            over_core(i)
            returned.append(i)

    def one_stage():
        if work:
            g, stages = work[0]
            next(stages)
            if computed:
                back(computed.pop(0))
            if g_left[g] == 1:
                work.pop(0)
                computed.append(g)
            g_left[g] -= 1

    g_left = [4] * len(groups)
    pass_on(0)
    rows[0, t] = fb[me]
    row_scales()
    for i in range(soon, n):
        dispatch(i)
    lag = 3
    for i in range(1, n + lag):
        if i < n:
            pass_on(i)
        if i == min(3, n - 1):
            pltpu.make_async_copy(wgud, wgud, wsem.at[1]).wait()
            arrived(scb.at[0 : n - 1], rsc.at[0])
        one_stage()
        if i >= lag:
            pass_over(i - lag)
            for g, group in enumerate(groups):
                if group[-1] == i - lag:
                    work.append((g, experts(g)))
        one_stage()
    while work:
        one_stage()
        if returned:
            over_y(returned.pop(0))
    for g in computed:
        back(g)
    for i in returned:
        over_y(i)
    arrived(r5.at[0 : n - 1], q5.at[0])

    finished = mid[...] + mm(wcomb[...], r5[...].reshape(n * cap, cw), 1, 0)
    outc[...] = finished.astype(BF16).reshape(nt, rows_here, cw)
    for i in range(1, nt):
        p = lax.rem(t + i, nt)
        send(outc.at[p], fin.at[t], sf.at[0], rf.at[0], {"tp": p})
    fin[t] = outc[t]
    arrived(fin.at[0 : nt - 1], rf.at[0])
    for p in range(nt):
        out[:, p * cw : (p + 1) * cw] = fin[p]
    departed(decall.at[:, 0 : size - 1], sd.at[0])
    departed(sbuf.at[:, 0 : size - 1], sa.at[0])
    departed(cbuf.at[:, 0 : size - 1], sb.at[0])
    departed(scols.at[0 : nt - 1], sst.at[0])
    departed(p1, sp1.at[0])
    departed(ph.at[0 : ny - 1], sp2.at[0])
    departed(squares.at[0 : nt - 1], su.at[0])
    departed(sca.at[0 : n - 1], ssc.at[0])
    departed(fb.at[0 : n - 1], sx.at[0])
    departed(hy.at[:, 0 : ny - 1], sy.at[0])
    departed(r4, sxc.at[0])
    departed(r4, s4.at[0])
    departed(hy.at[:, 0 : ny - 1], s6.at[0])
    departed(hb.at[0 : n - 1], s5.at[0])
    departed(outc.at[0 : nt - 1], sf.at[0])

    @pl.when(team < teams - 1)
    def _():
        departed(tsend, stt.at[0])


def solution(mesh):
    n, nt = mesh.shape["sp"], mesh.shape["tp"]
    ny = nt // 2

    def body(
        stream_in, queries, key_rows, values, decay_low, decay_matrix, decay_bias, decay_shift,
        head_gain, output_matrix, feed_gain, routes, route_weights, expert_gate, specialist_widen,
        expert_down,
    ):
        length, keys = queries.shape
        vals = values.shape[1]
        rows_here, width = stream_in.shape
        hidden = expert_gate.shape[2]
        cap = nt * max(1, TOP * length // (n * nt))
        cw = width // nt
        sides = cw // min(256, cw)
        step = max(1, min(n, 256 // cap))
        groups = n // step + 1
        size = next(x for x in ((4, 2, 1) if n > 8 else (2, 1)) if n % x == 0)
        pieces = (HV // size) // max(16, HV // size // PIECES)
        heads = keys // HK
        blocks = length // BLK
        vm = pltpu.VMEM
        dma = pltpu.SemaphoreType.DMA
        scratch = [
            vm((length, keys), F32), vm((max(1, blocks - 1), HV, keys), BF16),
            *[vm((heads, size, HV // size, HK), BF16)] * 4,
            *[vm((heads, HV // size, HK), BF16)] * 2,
            vm((heads, 1, HK), F32), vm((heads, size, 1, HK), F32),
            vm((length, vals), F32), vm((length, keys), BF16),
            vm(output_matrix.shape, BF16), vm((3, hidden, width), BF16), vm((length, vals), BF16),
            vm((nt, rows_here, cw), BF16), vm((ny, 2, length, cw), BF16), *[vm((ny, length, cw), BF16)] * 3,
            vm((length, cw), F32), vm((nt, 1, length), F32),
            vm((n * cap, length), BF16), vm((length, n * cap), BF16),
            vm((n, 1, 128), F32), vm((n, 1, 128), F32),
            vm((n, cap, cw), BF16), vm((n, nt, cap, cw), BF16),
            vm((step * cap, hidden), F32), vm((step * cap, hidden), BF16),
            vm((n, ny, 2, cap, cw), BF16), *[vm((n, ny, cap, cw), BF16)] * 3,
            vm((n, cap, cw), BF16), vm((n, cap, cw), BF16),
            vm((nt, rows_here, cw), BF16), vm((nt, rows_here, cw), BF16),
            dma((2,)),
            dma((1,)), dma((heads, pieces)), dma((1,)), dma((heads,)),
            dma((1,)), dma((heads,)), dma((1,)), dma((heads, pieces)),
            dma((1,)), dma((1,)), dma((1,)), dma((sides, ny)), dma((1,)), dma((sides, ny)),
            dma((1,)), dma((1,)), dma((1,)), dma((1,)),
            dma((1,)), dma((n,)), dma((1,)), dma((n, ny - 1)), dma((1,)), dma((groups,)),
            dma((1,)), dma((groups,)), dma((1,)), dma((n, ny - 1)), dma((1,)), dma((1,)),
            dma((1,)), dma((1,)),
        ]
        near = pl.BlockSpec(memory_space=pltpu.VMEM)
        far = pl.BlockSpec(memory_space=pl.ANY)
        return pl.pallas_call(
            functools.partial(layer_kernel, n, nt, cap, size),
            out_shape=jax.ShapeDtypeStruct((rows_here, width), BF16),
            in_specs=[near] * 9 + [far] + [near] * 3 + [far] * 3,
            out_specs=near,
            scratch_shapes=scratch,
            compiler_params=pltpu.CompilerParams(
                collective_id=0, has_side_effects=True, vmem_limit_bytes=64_000_000
            ),
            name="layer",
        )(
            stream_in, queries, key_rows, values, decay_low.T, decay_matrix, decay_bias.reshape(1, -1),
            decay_shift.T, head_gain.reshape(1, -1), output_matrix, feed_gain.reshape(1, -1), routes.T,
            route_weights.T, expert_gate.swapaxes(1, 2), specialist_widen.swapaxes(1, 2), expert_down,
        )

    return jax.shard_map(
        body,
        mesh=mesh,
        in_specs=(
            P(("sp", "tp"), None), P("sp", "tp"), P("sp", "tp"), P("sp", "tp"), P("sp", None),
            P(None, "tp"), P("tp"), P("sp", "tp"), P(), P("tp", None), P(), P("sp", None),
            P("sp", None), P("sp", None, "tp"), P("sp", None, "tp"), P("sp", "tp", None),
        ),
        out_specs=P(("sp", "tp"), None),
        check_vma=False,
    )
```

time: 102 us -> 93 us (0.912)
  Pallas kernels: 99.8 us -> 91.1 us
    pallas_call x1, Pallas kernels: 99.8 us -> 91.1 us  [body(): pl.pallas_call(functools.partial(layer_kernel, n, nt, cap, size), out_sha...]
where the time goes in v2:
time: 93 us; the launch traced here: 92.8 us
  Pallas kernels  91.1 us (98%)
  local copies, waits for them, and re-layouts  1.67 us (2%)
    pallas_call x1, Pallas kernels, body(): pl.pallas_call(functools.partial(layer_kernel, n, nt, cap, size), out_sha...  91.1 us

profile of v2, /device:TPU:1, one launch (start us, length us, event | category | flops | bytes accessed | tf_op | source)
XLA Modules:
  0.0 92.8 jit_solution(6308785350367857469)
XLA Ops:
  0.0 91.1 %layer.1 = bf16[64,2048]{1,0:T(8,128)(2,1)} custom-call(bf16[64,2048]{1,0:T(8,128)(2,1)} %stream.1, bf16[256,1024]{1,0:T(8,128)(2,1)} %q.1, bf16[256,1024]{1,0:T(8,128)(2,1)} %k.1, bf16[256,2048]{1,0:T(8,128)(2,1)} %v.1, bf16[16,256]{1,0:T(8,128)(2,1)} %bitcast.11, bf16[16,1024]{1,0:T(8,128)(2,1)} %mat.1, f32[1,1024]{1,0:T(1,128)} %bitcast.13, ...), custom_call_target="tpu_custom_call" | custom-call | tf_op jit(solution)/shard_map/layer/pallas_call | solution.py:487
  91.1 1.7 %copy.18 = bf16[64,2048]{1,0:T(8,128)(2,1)} copy(bf16[64,2048]{1,0:T(8,128)(2,1)} %layer.1) | data formatting | bytes 524288

commit v3 on v2

--- a/solution.py
+++ b/solution.py
@@ -34,13 +34,15 @@
 
 def layer_kernel(
     n, nt, cap, size,
-    stream, q, k, v, low, mat, bias, shift, gain, wout, fgain, routes, rweights, wgate, wup, wdown,
+    stream_in, q_in, k_in, v_in, low_in, mat_in, bias_in, shift_in, gain_in, wout, fgain_in, routes_in,
+    rweights_in, wgate, wup, wdown,
     out,
+    stream, q, k, v, low, mat, bias, shift, gain, fgain, routes, rweights,
     ins, prior, sbuf, rbuf, cbuf, carry, tsend, trecv, dec, decall, acc, qs,
-    wo, wgud, mixed,
-    scols, prod, p1, ph, p2, mid, squares, selt, wcomb, sca, scb,
+    wo, wgud, wt, mixed,
+    scols, prod, p1, ph, p2, mid, selt, wcomb, sca, scb,
     fb, rows, gates, hiddens, pb, r4, hy, r6, hb, r5, outc, fin,
-    wsem, sa, ra, sd, rd, sb, rb, stt, rtt, sst, rst, sp1, rp1, sp2, rp2, su, ru, ssc, rsc,
+    wsem, lsem, sa, ra, sd, rd, sb, rb, stt, rtt, sst, rst, sp1, rp1, sp2, rp2, ssc, rsc,
     sx, rx, sy, ry, sxc, rxc, s4, q4, s6, q6, s5, q5, sf, rf,
 ):
     me = lax.axis_index("sp")
@@ -75,12 +77,26 @@
     def columns(p, f=0, wide=tile):
         return pl.ds(pl.multiple_of(p * cw + f * tile, tile), wide)
 
+    total_devices = n * nt
+    rank = me * nt + t
     barrier = pltpu.get_barrier_semaphore()
-    for i in range(1, n):
-        pl.semaphore_signal(barrier, inc=1, device_id={"sp": lax.rem(me + i, n)}, device_id_type=MESH)
-    for i in range(1, nt):
-        pl.semaphore_signal(barrier, inc=1, device_id={"tp": lax.rem(t + i, nt)}, device_id_type=MESH)
-
+
+    @pl.loop(1, total_devices)
+    def _(i):
+        other = lax.rem(rank + i, total_devices)
+        there = {"sp": other // nt, "tp": lax.rem(other, nt)}
+        pl.semaphore_signal(barrier, inc=1, device_id=there, device_id_type=MESH)
+
+    loads = [
+        pltpu.make_async_copy(source, target, lsem.at[i])
+        for i, (source, target) in enumerate((
+            (low_in, low), (mat_in, mat), (bias_in, bias), (shift_in, shift), (k_in, k), (v_in, v),
+            (stream_in, stream), (q_in, q), (routes_in, routes), (rweights_in, rweights), (gain_in, gain),
+            (fgain_in, fgain),
+        ))
+    ]
+    for load in loads:
+        load.start()
     load_out = pltpu.make_async_copy(wout, wo, wsem.at[0])
     load_out.start()
     for i, weight in enumerate((wgate, wup, wdown)):
@@ -91,12 +107,17 @@
     causal = row_id >= col_id
     tril = causal.astype(F32)
 
+    for load in loads[:4]:
+        load.wait()
     shifts = shift[...].T
 
     for h in range(heads):
         ks, vs = slice(h * HK, (h + 1) * HK), slice(h * HV, (h + 1) * HV)
         pre = mm(low[...], mat[:, ks], 0, 0) + bias[:, ks]
         logged = (jnp.minimum(pre, 0.0) - jnp.log1p(jnp.exp(-jnp.abs(pre)))) / TEMPER + shifts[:, h : h + 1]
+        if h == 0:
+            for load in loads[4:6]:
+                load.wait()
         whole = None
         state = None
         for b in range(blocks):
@@ -113,7 +134,7 @@
         sbuf[h] = state.astype(BF16).reshape(size, HV // size, HK)
         dec[h] = jnp.exp(whole)
         if h == 0:
-            pl.semaphore_wait(barrier, n - 1 + nt - 1)
+            pl.semaphore_wait(barrier, total_devices - 1)
         for i in range(1, size):
             to = lax.rem(mine + i, size)
             send(dec.at[h], decall.at[h, mine], sd.at[0], rd.at[h], {"sp": first_one + to})
@@ -126,11 +147,14 @@
         rbuf[h, mine] = sbuf[h, mine]
         decall[h, mine] = dec[h]
 
+    for load in loads[6:]:
+        load.wait()
     for i in range(1, nt):
         to = lax.rem(t + i, nt)
         send(stream.at[:, columns(to, 0, cw)], scols.at[t], sst.at[0], rst.at[0], {"tp": to})
     scols[t] = stream[:, columns(t, 0, cw)]
 
+    turns = [(j, slice(a, a + 256)) for j in range(2) for a in range(0, width, 256)]
     onward = {"sp": lax.rem(me + size, n)}
     for h in range(heads):
         ks, vs = slice(h * HK, (h + 1) * HK), slice(h * HV, (h + 1) * HV)
@@ -179,6 +203,11 @@
                 local = local + mm((qf * jnp.exp(inside)).astype(BF16), prior[b - 1, :, ks], 1, 1)
             passed = last if passed is None else passed + last
             acc[at, vs] = local
+        if h == 0:
+            pltpu.make_async_copy(wgud, wgud, wsem.at[1]).wait()
+        if h < max(1, heads - 1):
+            for j, at in turns[h :: max(1, heads - 1)]:
+                wt[j, at, :] = wgud[j, :, at].T
         if h == min(1, heads - 1):
             lane = lax.broadcasted_iota(jnp.int32, (length, n), 1).astype(F32)
             named = routes[...].astype(F32).T
@@ -253,8 +282,27 @@
         x = scols[:, :, at].reshape(length, tile).astype(F32) + total
         mid[:, at] = x
         square = square + jnp.sum(x * x, axis=1, keepdims=True)
+        if f == len(sides) - 1:
+            row = jnp.broadcast_to(square, (length, 128)).T[0:8, :]
+            upper = row.astype(BF16).astype(F32)
+            middle = (row - upper).astype(BF16).astype(F32)
+            line = lax.broadcasted_iota(jnp.int32, (8, length), 0)
+            parts = jnp.where(line == 0, upper, jnp.where(line == 1, middle, jnp.where(line == 2, row - upper - middle, 0.0)))
+            slot_squares = jnp.sum(mm(parts.astype(BF16), selt[...], 1, 1), axis=0, keepdims=True)
+            for e in range(n):
+                sca[e, :, 0:cap] = slot_squares[:, e * cap : (e + 1) * cap]
+            for i in range(n):
+                to = lax.rem(me + i, n)
+                for j in range(0 if i else 1, nt):
+                    send(
+                        sca.at[to], scb.at[i * nt + t], ssc.at[0], rsc.at[0], {"sp": to, "tp": lax.rem(t + j, nt)}
+                    )
+            scb[t] = sca[me]
         picked = mm(selt[...], (x * fgain[:, columns(t, f)]).astype(BF16), 1, 0)
         fb[:, :, at] = picked.astype(BF16).reshape(n, cap, tile)
+        for i in range(1, n):
+            to = lax.rem(me + i, n)
+            send(fb.at[to, :, at], rows.at[i, t, :, at], sx.at[0], rx.at[i], {"sp": to})
 
     step = max(1, min(n, 256 // cap))
     groups = [range(a, a + step) for a in range(0, n, step)]
@@ -280,56 +328,32 @@
             arrived(block, ry.at[i, d - 1])
             send(block, block, sxc.at[0], rxc.at[group_of(i)], partner)
 
-    def dispatch(i):
-        to = lax.rem(me + i, n)
-        send(fb.at[to], rows.at[i, t], sx.at[0], rx.at[i], {"sp": to})
-
-    soon = min(4, n)
-    for i in range(1, soon):
-        dispatch(i)
-    squares[t] = jnp.broadcast_to(square, (length, 128)).T[0:1, :]
-    for i in range(1, nt):
-        p = lax.rem(t + i, nt)
-        send(squares.at[t], squares.at[t], su.at[0], ru.at[0], {"tp": p})
-
-    def row_scales():
-        arrived(squares.at[0 : nt - 1], ru.at[0])
-        total = jnp.sum(squares[...], axis=0)
-        scale = lax.rsqrt(total / width + EPSILON)
-        high = scale.astype(BF16).astype(F32)
-        middle = (scale - high).astype(BF16).astype(F32)
-        third = scale - high - middle
-        line = lax.broadcasted_iota(jnp.int32, (8, length), 0)
-        parts = jnp.where(line == 0, high, jnp.where(line == 1, middle, jnp.where(line == 2, third, 0.0)))
-        slot_scale = jnp.sum(mm(parts.astype(BF16), selt[...], 1, 1), axis=0, keepdims=True)
-        for e in range(n):
-            sca[e, :, 0:cap] = slot_scale[:, e * cap : (e + 1) * cap]
-        for i in range(1, n):
-            to = lax.rem(me + i, n)
-            send(sca.at[to], scb.at[i], ssc.at[0], rsc.at[0], {"sp": to})
-        scb[0] = sca[me]
-
     def experts(g):
         group = groups[g]
         span = slice(group[0], group[-1] + 1)
         size_here = len(group) * cap
         arrived(rows.at[span, 0:ny], rxc.at[g])
-        scales = [jnp.broadcast_to(scb[i], (8, 128)).T[0:cap, 0:1] for i in group]
-        scale = jnp.concatenate(scales, axis=0)
         parts = [rows[span, p].reshape(size_here, cw) for p in range(nt)]
-        gates[0:size_here] = mm(jnp.concatenate(parts, axis=1), wgud[0], 1, 1) * scale
+        gates[0:size_here] = mm(jnp.concatenate(parts, axis=1), wt[0], 1, 0)
         yield
         parts = [rows[span, p].reshape(size_here, cw) for p in range(nt)]
-        lifted = mm(jnp.concatenate(parts, axis=1), wgud[1], 1, 1) * scale
-        gated = gates[0:size_here]
+        lifted = mm(jnp.concatenate(parts, axis=1), wt[1], 1, 0)
+        if g == 0:
+            arrived(scb.at[0 : n * nt - 1], rsc.at[0])
+        scales = []
+        for i in group:
+            total = jnp.sum(scb[i * nt : (i + 1) * nt], axis=0)
+            line = lax.rsqrt(total / width + EPSILON)
+            scales.append(jnp.broadcast_to(line, (8, 128)).T[0:cap, 0:1])
+        scale = jnp.concatenate(scales, axis=0)
+        lifted = lifted * scale
+        gated = gates[0:size_here] * scale
         hiddens[0:size_here] = (gated * jax.nn.sigmoid(gated) * lifted).astype(BF16)
         yield
         for core in (1 - c, c):
-            @pl.loop(0, ny)
-            def _(d):
+            for d in range(ny):
                 piece = mm(hiddens[0:size_here], wgud[2, :, columns(2 * d + core, 0, cw)], 1, 0).astype(BF16)
                 pb[span, d, core] = piece.reshape(len(group), cap, cw)
-
             if core is not c:
                 for i in group:
                     for d in range(ny):
@@ -364,10 +388,10 @@
 
     def one_stage():
         if work:
+            if computed:
+                back(computed.pop(0))
             g, stages = work[0]
             next(stages)
-            if computed:
-                back(computed.pop(0))
             if g_left[g] == 1:
                 work.pop(0)
                 computed.append(g)
@@ -376,16 +400,10 @@
     g_left = [4] * len(groups)
     pass_on(0)
     rows[0, t] = fb[me]
-    row_scales()
-    for i in range(soon, n):
-        dispatch(i)
     lag = 3
     for i in range(1, n + lag):
         if i < n:
             pass_on(i)
-        if i == min(3, n - 1):
-            pltpu.make_async_copy(wgud, wgud, wsem.at[1]).wait()
-            arrived(scb.at[0 : n - 1], rsc.at[0])
         one_stage()
         if i >= lag:
             pass_over(i - lag)
@@ -418,8 +436,7 @@
     departed(scols.at[0 : nt - 1], sst.at[0])
     departed(p1, sp1.at[0])
     departed(ph.at[0 : ny - 1], sp2.at[0])
-    departed(squares.at[0 : nt - 1], su.at[0])
-    departed(sca.at[0 : n - 1], ssc.at[0])
+    departed(scb.at[0 : n * nt - 1], ssc.at[0])
     departed(fb.at[0 : n - 1], sx.at[0])
     departed(hy.at[:, 0 : ny - 1], sy.at[0])
     departed(r4, sxc.at[0])
@@ -457,27 +474,33 @@
         blocks = length // BLK
         vm = pltpu.VMEM
         dma = pltpu.SemaphoreType.DMA
+        given = [
+            stream_in, queries, key_rows, values, decay_low.T, decay_matrix, decay_bias.reshape(1, -1),
+            decay_shift.T, head_gain.reshape(1, -1), output_matrix, feed_gain.reshape(1, -1), routes.T,
+            route_weights.T, expert_gate.swapaxes(1, 2), specialist_widen.swapaxes(1, 2), expert_down,
+        ]
         scratch = [
+            *[vm(given[i].shape, given[i].dtype) for i in (0, 1, 2, 3, 4, 5, 6, 7, 8, 10, 11, 12)],
             vm((length, keys), F32), vm((max(1, blocks - 1), HV, keys), BF16),
             *[vm((heads, size, HV // size, HK), BF16)] * 4,
             *[vm((heads, HV // size, HK), BF16)] * 2,
             vm((heads, 1, HK), F32), vm((heads, size, 1, HK), F32),
             vm((length, vals), F32), vm((length, keys), BF16),
-            vm(output_matrix.shape, BF16), vm((3, hidden, width), BF16), vm((length, vals), BF16),
+            vm(output_matrix.shape, BF16), vm((3, hidden, width), BF16), vm((2, width, hidden), BF16), vm((length, vals), BF16),
             vm((nt, rows_here, cw), BF16), vm((ny, 2, length, cw), BF16), *[vm((ny, length, cw), BF16)] * 3,
-            vm((length, cw), F32), vm((nt, 1, length), F32),
+            vm((length, cw), F32),
             vm((n * cap, length), BF16), vm((length, n * cap), BF16),
-            vm((n, 1, 128), F32), vm((n, 1, 128), F32),
+            vm((n, 1, 128), F32), vm((n * nt, 1, 128), F32),
             vm((n, cap, cw), BF16), vm((n, nt, cap, cw), BF16),
             vm((step * cap, hidden), F32), vm((step * cap, hidden), BF16),
             vm((n, ny, 2, cap, cw), BF16), *[vm((n, ny, cap, cw), BF16)] * 3,
             vm((n, cap, cw), BF16), vm((n, cap, cw), BF16),
             vm((nt, rows_here, cw), BF16), vm((nt, rows_here, cw), BF16),
-            dma((2,)),
+            dma((2,)), dma((12,)),
             dma((1,)), dma((heads, pieces)), dma((1,)), dma((heads,)),
             dma((1,)), dma((heads,)), dma((1,)), dma((heads, pieces)),
             dma((1,)), dma((1,)), dma((1,)), dma((sides, ny)), dma((1,)), dma((sides, ny)),
-            dma((1,)), dma((1,)), dma((1,)), dma((1,)),
+            dma((1,)), dma((1,)),
             dma((1,)), dma((n,)), dma((1,)), dma((n, ny - 1)), dma((1,)), dma((groups,)),
             dma((1,)), dma((groups,)), dma((1,)), dma((n, ny - 1)), dma((1,)), dma((1,)),
             dma((1,)), dma((1,)),
@@ -487,18 +510,14 @@
         return pl.pallas_call(
             functools.partial(layer_kernel, n, nt, cap, size),
             out_shape=jax.ShapeDtypeStruct((rows_here, width), BF16),
-            in_specs=[near] * 9 + [far] + [near] * 3 + [far] * 3,
+            in_specs=[far] * 16,
             out_specs=near,
             scratch_shapes=scratch,
             compiler_params=pltpu.CompilerParams(
                 collective_id=0, has_side_effects=True, vmem_limit_bytes=64_000_000
             ),
             name="layer",
-        )(
-            stream_in, queries, key_rows, values, decay_low.T, decay_matrix, decay_bias.reshape(1, -1),
-            decay_shift.T, head_gain.reshape(1, -1), output_matrix, feed_gain.reshape(1, -1), routes.T,
-            route_weights.T, expert_gate.swapaxes(1, 2), specialist_widen.swapaxes(1, 2), expert_down,
-        )
+        )(*given)
 
     return jax.shard_map(
         body,

time: 93 us -> 86.9 us (0.934)
  Pallas kernels: 91.1 us -> 85 us
    pallas_call x1, Pallas kernels: 91.1 us -> 85 us  [body(): pl.pallas_call(functools.partial(layer_kernel, n, nt, cap, size), out_sha...]
where the time goes in v3:
time: 86.9 us; the launch traced here: 86.7 us
  Pallas kernels  85 us (98%)
  local copies, waits for them, and re-layouts  1.67 us (2%)
    pallas_call x1, Pallas kernels, body(): pl.pallas_call(functools.partial(layer_kernel, n, nt, cap, size), out_sha...  85 us

profile of v3, /device:TPU:1, one launch (start us, length us, event | category | flops | bytes accessed | tf_op | source)
XLA Modules:
  0.0 86.7 jit_solution(17750374155302048702)
XLA Ops:
  0.0 85.0 %layer.1 = bf16[64,2048]{1,0:T(8,128)(2,1)} custom-call(bf16[64,2048]{1,0:T(8,128)(2,1)} %stream_in.1, bf16[256,1024]{1,0:T(8,128)(2,1)} %q_in.1, bf16[256,1024]{1,0:T(8,128)(2,1)} %k_in.1, bf16[256,2048]{1,0:T(8,128)(2,1)} %v_in.1, bf16[16,256]{1,0:T(8,128)(2,1)} %bitcast.11, bf16[16,1024]{1,0:T(8,128)(2,1)} %mat_in.1, f32[1,1024]{1,0:T(1,128)} %bitcast.13, ...), custom_call_target="tpu_custom_call" | custom-call | tf_op jit(solution)/shard_map/layer/pallas_call | solution.py:510
  85.0 1.7 %copy.18 = bf16[64,2048]{1,0:T(8,128)(2,1)} copy(bf16[64,2048]{1,0:T(8,128)(2,1)} %layer.1) | data formatting | bytes 524288

commit v4 on v3

--- a/solution.py
+++ b/solution.py
@@ -295,14 +295,14 @@
                 to = lax.rem(me + i, n)
                 for j in range(0 if i else 1, nt):
                     send(
-                        sca.at[to], scb.at[i * nt + t], ssc.at[0], rsc.at[0], {"sp": to, "tp": lax.rem(t + j, nt)}
+                        sca.at[to], scb.at[me * nt + t], ssc.at[0], rsc.at[0], {"sp": to, "tp": lax.rem(t + j, nt)}
                     )
-            scb[t] = sca[me]
+            scb[me * nt + t] = sca[me]
         picked = mm(selt[...], (x * fgain[:, columns(t, f)]).astype(BF16), 1, 0)
         fb[:, :, at] = picked.astype(BF16).reshape(n, cap, tile)
         for i in range(1, n):
             to = lax.rem(me + i, n)
-            send(fb.at[to, :, at], rows.at[i, t, :, at], sx.at[0], rx.at[i], {"sp": to})
+            send(fb.at[to, :, at], rows.at[me, t, :, at], sx.at[0], rx.at[me], {"sp": to})
 
     step = max(1, min(n, 256 // cap))
     groups = [range(a, a + step) for a in range(0, n, step)]
@@ -313,13 +313,23 @@
     def group_of(i):
         return next(g for g, group in enumerate(groups) if i in group)
 
-    def pass_on(i):
-        if i > 0:
-            arrived(rows.at[i, t], rx.at[i])
-        block = fb.at[me] if i == 0 else rows.at[i, t]
+    def group_at(i):
+        g = 0
+        for group in groups[1:]:
+            g = g + (i >= group[0]).astype(jnp.int32)
+        return g
+
+    def forward(i, g):
+        block = rows.at[i, t]
         for d in range(1, ny):
             send(block, rows.at[i, t], sy.at[0], ry.at[i, d - 1], {"tp": 2 * lax.rem(y + d, ny) + c})
-        send(block, rows.at[i, t], sxc.at[0], rxc.at[group_of(i)], partner)
+        send(block, rows.at[i, t], sxc.at[0], rxc.at[g], partner)
+
+    def pass_on(i):
+        @pl.when(i // size != team)
+        def _():
+            arrived(rows.at[i, t], rx.at[i])
+            forward(i, group_of(i))
 
     def pass_over(i):
         for d in range(1, ny):
@@ -371,12 +381,16 @@
         for d in range(1, ny):
             arrived(r6.at[i, d], q6.at[i, d - 1])
             both = both + r6[i, d].astype(F32)
-        if i == 0:
-            r5[me] = both.astype(BF16)
-        else:
-            j = lax.rem(me + n - i, n)
-            hb[i] = both.astype(BF16)
-            send(hb.at[i], r5.at[me], s5.at[0], q5.at[0], {"sp": j})
+        hb[i] = both.astype(BF16)
+
+        @pl.when(i == me)
+        def _():
+            r5[me] = hb[i]
+
+        @pl.when(i != me)
+        def _():
+            send(hb.at[i], r5.at[me], s5.at[0], q5.at[0], {"sp": i})
+
 
     work, computed, returned = [], [], []
 
@@ -398,10 +412,14 @@
             g_left[g] -= 1
 
     g_left = [4] * len(groups)
-    pass_on(0)
-    rows[0, t] = fb[me]
+    rows[me, t] = fb[me]
+    forward(me, group_at(me))
+    for i in range(1, size):
+        mate = first_one + lax.rem(mine + i, size)
+        arrived(rows.at[mate, t], rx.at[mate])
+        forward(mate, group_at(mate))
     lag = 3
-    for i in range(1, n + lag):
+    for i in range(n + lag):
         if i < n:
             pass_on(i)
         one_stage()
@@ -509,7 +527,7 @@
         far = pl.BlockSpec(memory_space=pl.ANY)
         return pl.pallas_call(
             functools.partial(layer_kernel, n, nt, cap, size),
-            out_shape=jax.ShapeDtypeStruct((rows_here, width), BF16),
+            out_shape=pltpu.VMEM((rows_here, width), BF16),
             in_specs=[far] * 16,
             out_specs=near,
             scratch_shapes=scratch,

time: 86.9 us -> 83.3 us (0.959)
  the two profiles are of different devices: /device:TPU:1 before, /device:TPU:31 now
where the time goes in v4:
time: 83.3 us; the launch traced here: 83.1 us
  Pallas kernels  82.4 us (99%)
    pallas_call x1, Pallas kernels, body(): pl.pallas_call(functools.partial(layer_kernel, n, nt, cap, size), out_sha...  82.4 us

profile of v4, /device:TPU:31, one launch (start us, length us, event | category | flops | bytes accessed | tf_op | source)
XLA Modules:
  0.0 83.1 jit_solution(11948558832265054797)
XLA Ops:
  0.0 82.4 %layer.1 = bf16[64,2048]{1,0:T(8,128)(2,1)S(1)} custom-call(bf16[64,2048]{1,0:T(8,128)(2,1)} %stream_in.1, bf16[256,1024]{1,0:T(8,128)(2,1)} %q_in.1, bf16[256,1024]{1,0:T(8,128)(2,1)} %k_in.1, bf16[256,2048]{1,0:T(8,128)(2,1)} %v_in.1, bf16[16,256]{1,0:T(8,128)(2,1)} %bitcast.11, bf16[16,1024]{1,0:T(8,128)(2,1)} %mat_in.1, f32[1,1024]{1,0:T(1,128)} %bitcast.13, ...), custom_call_target="tpu_custom_call" | custom-call | tf_op jit(solution)/shard_map/layer/pallas_call | solution.py:528
  82.4 0.7 copy.18

commit v5 on v4

--- a/solution.py
+++ b/solution.py
@@ -282,6 +282,11 @@
         x = scols[:, :, at].reshape(length, tile).astype(F32) + total
         mid[:, at] = x
         square = square + jnp.sum(x * x, axis=1, keepdims=True)
+        picked = mm(selt[...], (x * fgain[:, columns(t, f)]).astype(BF16), 1, 0)
+        fb[:, :, at] = picked.astype(BF16).reshape(n, cap, tile)
+        for i in range(1, n):
+            to = lax.rem(me + i, n)
+            send(fb.at[to, :, at], rows.at[me, t, :, at], sx.at[0], rx.at[me], {"sp": to})
         if f == len(sides) - 1:
             row = jnp.broadcast_to(square, (length, 128)).T[0:8, :]
             upper = row.astype(BF16).astype(F32)
@@ -298,11 +303,6 @@
                         sca.at[to], scb.at[me * nt + t], ssc.at[0], rsc.at[0], {"sp": to, "tp": lax.rem(t + j, nt)}
                     )
             scb[me * nt + t] = sca[me]
-        picked = mm(selt[...], (x * fgain[:, columns(t, f)]).astype(BF16), 1, 0)
-        fb[:, :, at] = picked.astype(BF16).reshape(n, cap, tile)
-        for i in range(1, n):
-            to = lax.rem(me + i, n)
-            send(fb.at[to, :, at], rows.at[me, t, :, at], sx.at[0], rx.at[me], {"sp": to})
 
     step = max(1, min(n, 256 // cap))
     groups = [range(a, a + step) for a in range(0, n, step)]
@@ -431,8 +431,6 @@
         one_stage()
     while work:
         one_stage()
-        if returned:
-            over_y(returned.pop(0))
     for g in computed:
         back(g)
     for i in returned:

time: 83.3 us -> 82.9 us (level)
  no operation moved by 1% of the time
where the time goes in v5:
time: 82.9 us; the launch traced here: 82.7 us
  Pallas kernels  81.9 us (99%)
    pallas_call x1, Pallas kernels, body(): pl.pallas_call(functools.partial(layer_kernel, n, nt, cap, size), out_sha...  81.9 us

profile of v5, /device:TPU:31, one launch (start us, length us, event | category | flops | bytes accessed | tf_op | source)
XLA Modules:
  0.0 82.7 jit_solution(12696538841287521400)
XLA Ops:
  0.0 81.9 %layer.1 = bf16[64,2048]{1,0:T(8,128)(2,1)S(1)} custom-call(bf16[64,2048]{1,0:T(8,128)(2,1)} %stream_in.1, bf16[256,1024]{1,0:T(8,128)(2,1)} %q_in.1, bf16[256,1024]{1,0:T(8,128)(2,1)} %k_in.1, bf16[256,2048]{1,0:T(8,128)(2,1)} %v_in.1, bf16[16,256]{1,0:T(8,128)(2,1)} %bitcast.11, bf16[16,1024]{1,0:T(8,128)(2,1)} %mat_in.1, f32[1,1024]{1,0:T(1,128)} %bitcast.13, ...), custom_call_target="tpu_custom_call" | custom-call | tf_op jit(solution)/shard_map/layer/pallas_call | solution.py:526
  82.0 0.7 copy.18
